TPU v7x, 512 devices: a whole 4x4x16 slice. The times are simulated.
512 devices in a mesh: fs: 128 (over z, x, core), tp: 4 (over y).
Axes of the slice: x: 4, y: 4, z: 16, core: 2. Of those that a mesh axis runs over, the one named last changes fastest.
Arguments:
- normed_input: bfloat16 [131072, 2048], P('fs'), may hold values from -64 to 64
- query_cotangent: bfloat16 [131072, 1024], P('fs', 'tp'), may hold values from -6 to 6
- key_cotangent: bfloat16 [131072, 512], P('fs', 'tp'), may hold values from -6 to 6
- query_weight: float32 [2048, 1024], P('fs', 'tp'), may hold values from -6 to 6
- key_weight: float32 [2048, 512], P('fs', 'tp'), may hold values from -6 to 6
- query_basis: bfloat16 [1024, 128], P('tp'), may hold values from -1 to 1
- key_basis: bfloat16 [512, 128], P('tp'), may hold values from -1 to 1
- moment_mean: float32 [2, 2048, 128], P(None, 'fs'), may hold values from -3 to 3
- moment_square: float32 [2, 2048, 128], P(None, 'fs'), may hold values from 0.25 to 4
Outputs:
- query_step: float32 [2048, 1024], P('fs', 'tp')
- key_step: float32 [2048, 512], P('fs', 'tp')
- query_updated: float32 [2048, 1024], P('fs', 'tp')
- key_updated: float32 [2048, 512], P('fs', 'tp')
- query_copy: bfloat16 [2048, 1024], P('fs', 'tp')
- key_copy: bfloat16 [2048, 512], P('fs', 'tp')
- mean_updated: float32 [2, 2048, 128], P(None, 'fs')
- square_updated: float32 [2, 2048, 128], P(None, 'fs')
All inputs are finite; a program needn't handle non-finite values.
Results may differ from a plain program's by a relative error of at most 0.0011.
Values sent between devices are 32-bit elements; how exact they have to be, the bound alone decides.
No kernel may reach another device: no remote copies, remote signals or barrier semaphores. Data moves between devices by JAX's collectives and lax.ppermute only.
A program may use at most 64 MiB of HBM per device.

v0:
```python
import jax
import jax.numpy as jnp
from jax import lax
from jax.sharding import Mesh
from jax.sharding import PartitionSpec as P

FS = ("fs_0", "fs_1", "fs_2")


BETA_MEAN = 0.75
BETA_SQUARE = 0.8
STEP_RATE = 0.25
EPSILON = 1e-06


def cut_along(shard, dim, size):
    before, after = (shard.shape[:dim], shard.shape[dim + 1 :])
    return jnp.moveaxis(shard.reshape(*before, size, -1, *after), dim, 0)


def sent_and_summed(shard, axis, dim):
    size = lax.axis_size(axis)
    blocks = lax.all_to_all(cut_along(shard, dim, size), axis, 0, 0, tiled=True)
    return jnp.sum(blocks, axis=0)


def summed_rows(shard, axes, dim):
    far, near = axes
    blocks = cut_along(shard, dim, lax.axis_size(far))
    nearer = sent_and_summed(blocks, near, dim + 1)
    arrived = lax.all_to_all(nearer, far, split_axis=0, concat_axis=0, tiled=True)
    return arrived.sum(axis=0)


def sent_to_all(shard, axis):
    size = lax.axis_size(axis)
    return lax.all_to_all(
        jnp.broadcast_to(shard[None], (size, *shard.shape)), axis, 0, 0, tiled=True
    )


def over_copies(shard, axis):
    everything = sent_to_all(shard, axis)
    return jnp.sum(everything, axis=0)


def over_axes(shard, axes):
    far, near = axes
    return over_copies(over_copies(shard, near), far)


def local(
    normed_input,
    query_cotangent,
    key_cotangent,
    query_weight,
    key_weight,
    query_basis,
    key_basis,
    moment_mean,
    moment_square,
):
    highest = lax.Precision.HIGHEST
    contract = (((0,), (0,)), ((), ()))
    row_count = query_weight.shape[0]
    rank_width = query_basis.shape[1]
    query_float = query_basis.astype(jnp.float32)
    key_float = key_basis.astype(jnp.float32)
    partial_precision = lax.Precision.HIGH
    query_part = lax.dot_general(
        normed_input, query_cotangent, contract, preferred_element_type=jnp.float32
    )
    key_part = lax.dot_general(
        normed_input, key_cotangent, contract, preferred_element_type=jnp.float32
    )
    query_part, key_part = (query_part, key_part)
    summed = summed_rows(
        jnp.concatenate(
            [
                jnp.dot(query_part, query_float, precision=partial_precision),
                jnp.dot(key_part, key_float, precision=partial_precision),
            ],
            axis=1,
        ),
        (("fs_0", "fs_1"), "fs_2"),
        0,
    )
    query_projected = summed[:, :rank_width]
    key_projected = summed[:, rank_width:]
    projected = over_copies(jnp.stack([query_projected, key_projected]), "tp")
    total_square = over_axes(jnp.sum(projected * projected), (("fs_0", "fs_1"), "fs_2"))
    entry_count = 2.0 * row_count * lax.axis_size(FS) * rank_width
    normalized = projected * lax.rsqrt(total_square / entry_count + EPSILON)
    mean_updated = BETA_MEAN * moment_mean + (1.0 - BETA_MEAN) * normalized
    square_updated = BETA_SQUARE * moment_square + (1.0 - BETA_SQUARE) * normalized * normalized
    direction = mean_updated / jnp.sqrt(square_updated)
    outer = (((1,), (1,)), ((), ()))
    query_step = lax.dot_general(direction[0], query_float, outer, precision=highest)
    key_step = lax.dot_general(direction[1], key_float, outer, precision=highest)
    query_updated = query_weight - STEP_RATE * query_step
    key_updated = key_weight - STEP_RATE * key_step
    return (
        query_step,
        key_step,
        query_updated,
        key_updated,
        query_updated.astype(jnp.bfloat16),
        key_updated.astype(jnp.bfloat16),
        mean_updated,
        square_updated,
    )


def solution(mesh):
    split = Mesh(mesh.devices.reshape(16, 4, 2, mesh.shape["tp"]), ("fs_0", "fs_1", "fs_2", "tp"))
    in_specs = (
        P(FS, None),
        P(FS, "tp"),
        P(FS, "tp"),
        P(FS, "tp"),
        P(FS, "tp"),
        P("tp", None),
        P("tp", None),
        P(None, FS, None),
        P(None, FS, None),
    )
    out_specs = (
        P(FS, "tp"),
        P(FS, "tp"),
        P(FS, "tp"),
        P(FS, "tp"),
        P(FS, "tp"),
        P(FS, "tp"),
        P(None, FS, None),
        P(None, FS, None),
    )
    return jax.shard_map(local, mesh=split, in_specs=in_specs, out_specs=out_specs, check_vma=False)
```

profile of v0, /device:TPU:1, one launch (start us, length us, event | category | flops | bytes accessed | tf_op | source)
XLA Modules:
  0.0 132.0 jit_solution(1930328877032753912)
XLA Ops:
  0.6 0.0 copy-start
  0.6 0.0 copy-start.1
  0.7 3.7 %fusion.8 = f32[2048,128]{1,0:T(8,128)S(1)} fusion(bf16[1024,2048]{1,0:T(8,128)(2,1)} %param.9, bf16[1024,128]{1,0:T(8,128)(2,1)} %param.11), kind=kOutput, calls=%fused_computation.19 | convolution fusion | flops 536870912 | bytes 5505024 | tf_op jit(solution)/shard_map/dot_general | solution.py:73
  4.3 0.0 copy-done
  4.3 0.0 copy-done.1
  4.3 0.0 copy-start.3
  4.3 1.4 %fusion.6 = f32[2048,256]{1,0:T(8,128)S(1)} fusion(bf16[1024,2048]{1,0:T(8,128)(2,1)S(1)} %copy-done.1, bf16[1024,256]{1,0:T(8,128)(2,1)S(1)} %copy-done), kind=kOutput, calls=%fused_computation.17 | convolution fusion | flops 1073741824 | bytes 6815744 | tf_op jit(solution)/shard_map/dot_general | solution.py:70
  5.7 0.0 copy-start.2
  5.7 0.5 fusion.9
  6.2 0.3 copy-done.2
  6.6 0.8 fusion.7
  7.4 0.1 pad_maximum_fusion
  7.6 1.9 %copy.22 = f32[2048,256]{1,0:T(8,128)} copy(f32[2048,256]{0,1:T(8,128)S(1)} %pad_maximum_fusion) | data formatting | bytes 4194304 | tf_op jit(solution)/shard_map/concatenate | solution.py:78
  9.4 1.8 %copy.23 = f32[2,64,16,256]{3,2,1,0:T(8,128)S(1)} copy(f32[2,64,16,256]{3,2,0,1:T(8,128)} %bitcast.27) | data formatting | bytes 4194304 | tf_op jit(solution)/shard_map/transpose | solution.py:18
  11.2 11.9 %all_to_all.27 = f32[2,64,16,256]{3,2,1,0:T(8,128)S(1)} all-to-all(f32[2,64,16,256]{3,2,1,0:T(8,128)S(1)} %copy.23), channel_id=1, replica_groups=mesh['fs_0'=16,'fs_1'=4,'fs_2'=2,'tp'=4] {'fs_2'}, dimensions={0} | all-to-all | bytes 4194304 | tf_op jit(solution)/shard_map/all_to_all | solution.py:23
  23.1 1.3 reduce_sum.54
  24.4 65.7 %all_to_all.28 = f32[64,16,256]{2,1,0:T(8,128)S(1)} all-to-all(f32[64,16,256]{2,1,0:T(8,128)} %reduce_sum.54), channel_id=1, replica_groups=mesh['fs_0'=16,'fs_1'=4,'fs_2'=2,'tp'=4] {'fs_0','fs_1'}, dimensions={0} | all-to-all | bytes 2097152 | tf_op jit(solution)/shard_map/all_to_all | solution.py:31
  90.1 0.1 reduce_sum.55
  90.2 8.5 %all_to_all.29 = f32[4,2,16,128]{3,2,1,0:T(8,128)S(1)} all-to-all(f32[4,2,16,128]{3,2,1,0:T(8,128)S(1)} %broadcast_in_dim.6), channel_id=1, replica_groups=mesh['fs_0'=16,'fs_1'=4,'fs_2'=2,'tp'=4] {'tp'}, dimensions={0} | all-to-all | bytes 131072 | tf_op jit(solution)/shard_map/all_to_all | solution.py:37
  98.7 0.6 multiply_reduce_fusion
  99.3 0.6 broadcast_in_dim.7
  99.9 8.4 %all_to_all.30 = f32[2,1,1]{2,1,0:T(1,128)S(1)} all-to-all(f32[2,1,1]{2,1,0:T(1,128)S(1)} %broadcast_in_dim.7), channel_id=1, replica_groups=mesh['fs_0'=16,'fs_1'=4,'fs_2'=2,'tp'=4] {'fs_2'}, dimensions={0} | all-to-all | bytes 16 | tf_op jit(solution)/shard_map/all_to_all | solution.py:37
  108.3 0.6 reduce_sum.58
  108.9 0.7 broadcast_in_dim.8
  109.6 18.8 %all_to_all.31 = f32[64,1,1]{2,1,0:T(1,128)S(1)} all-to-all(f32[64,1,1]{2,1,0:T(1,128)S(1)} %broadcast_in_dim.8), channel_id=1, replica_groups=mesh['fs_0'=16,'fs_1'=4,'fs_2'=2,'tp'=4] {'fs_0','fs_1'}, dimensions={0} | all-to-all | bytes 512 | tf_op jit(solution)/shard_map/all_to_all | solution.py:37
  128.4 0.7 reduce_sum.59
  129.8 0.0 copy-done.4
  129.8 0.0 copy-done.5
  129.8 0.6 rsqrt_multiply_fusion
  130.4 0.0 copy-done.7
  130.4 0.8 fusion.3
  131.2 0.8 fusion.4
  (10 shorter events, 0.0 us)
Async XLA Ops:
  0.6 3.7 %copy-start = (bf16[1024,256]{1,0:T(8,128)(2,1)S(1)}, bf16[1024,256]{1,0:T(8,128)(2,1)}, u32[]{:S(2)}) copy-start(bf16[1024,256]{1,0:T(8,128)(2,1)} %param.10) | copy-start | bytes 1572868
  0.6 3.7 %copy-start.1 = (bf16[1024,2048]{1,0:T(8,128)(2,1)S(1)}, bf16[1024,2048]{1,0:T(8,128)(2,1)}, u32[]{:S(2)}) copy-start(bf16[1024,2048]{1,0:T(8,128)(2,1)} %param.9) | copy-start | bytes 12582916
  4.3 1.4 %copy-start.3 = (bf16[128,128]{1,0:T(8,128)(2,1)S(1)}, bf16[128,128]{1,0:T(8,128)(2,1)}, u32[]{:S(2)}) copy-start(bf16[128,128]{1,0:T(8,128)(2,1)} %param.15) | copy-start | bytes 98308
  5.7 0.8 copy-start.2
  24.3 105.4 %copy-start.4 = (f32[2,16,128]{2,1,0:T(8,128)S(1)}, f32[2,16,128]{2,1,0:T(8,128)}, u32[]{:S(2)}) copy-start(f32[2,16,128]{2,1,0:T(8,128)} %param.17) | copy-start | bytes 49156
  24.4 105.4 %copy-start.5 = (f32[2,16,128]{2,1,0:T(8,128)S(1)}, f32[2,16,128]{2,1,0:T(8,128)}, u32[]{:S(2)}) copy-start(f32[2,16,128]{2,1,0:T(8,128)} %param.16) | copy-start | bytes 49156
  24.4 106.1 %copy-start.7 = (f32[16,128]{1,0:T(8,128)S(1)}, f32[16,128]{1,0:T(8,128)}, u32[]{:S(2)}) copy-start(f32[16,128]{1,0:T(8,128)} %param.13) | copy-start | bytes 24580
  24.4 106.9 %copy-start.6 = (f32[16,256]{1,0:T(8,128)S(1)}, f32[16,256]{1,0:T(8,128)}, u32[]{:S(2)}) copy-start(f32[16,256]{1,0:T(8,128)} %param.12) | copy-start | bytes 49156
where the time goes:
time: 132 us
  blocking collectives  113 us (86%)
  matrix products  7.92 us (6%)
  local copies, waits for them, and re-layouts  5.35 us (4%)
  other arithmetic  3.99 us (3%)
  between operations  1.48 us (1%)
    all_to_all x1, blocking collectives, summed_rows(): lax.all_to_all(nearer, far, split_axis=0, concat_axis=0, tiled=True)  65.7 us
    all_to_all x3, blocking collectives, sent_to_all(): lax.all_to_all(jnp.broadcast_to(shard[None], (size, *shard.shape)), axis,...  35.7 us
    all_to_all x1, blocking collectives, sent_and_summed(): blocks = lax.all_to_all(cut_along(shard, dim, size), axis, 0, 0, tiled=True)  11.9 us
    dot_general x1, matrix products, local(): lax.dot_general(normed_input, key_cotangent, contract, preferred_element_...  3.65 us

commit v1 on v0

v1 whole, which is shorter than its diff:
```python
import jax
import jax.numpy as jnp
from jax import lax
from jax.experimental import pallas as pl
from jax.experimental.pallas import tpu as pltpu
from jax.sharding import Mesh
from jax.sharding import PartitionSpec as P

FS = ("fs_0", "fs_1", "fs_2")

BETA_MEAN = 0.75
BETA_SQUARE = 0.8
STEP_RATE = 0.25
EPSILON = 1e-06
BLOCK = 256

HIGHEST = lax.Precision.HIGHEST
OUTER = (((1,), (1,)), ((), ()))
TOKENS_OUT = (((0,), (0,)), ((), ()))


def dot(a, b, dims, precision=None):
    return lax.dot_general(a, b, dims, precision=precision, preferred_element_type=jnp.float32)


def halves(value):
    high = value.astype(jnp.bfloat16)
    low = (value - high.astype(jnp.float32)).astype(jnp.bfloat16)
    return high, low


def store_block(x_ref, factor, out_ref):
    both = dot(x_ref[...], factor, TOKENS_OUT)
    rank = both.shape[1] // 2
    part = both[:, :rank] + both[:, rank:]
    zs, rows = out_ref.shape[1], out_ref.shape[0] * out_ref.shape[2]
    for z in range(zs):
        piece = part[z * rows : (z + 1) * rows]
        out_ref[:, z, :, :] = piece.reshape(out_ref.shape[0], out_ref.shape[2], rank)


def other_kernel(core, cq_ref, ck_ref, bq_ref, bk_ref, x_ref, out_ref, own_ref, other_ref):
    @pl.when(pl.program_id(0) == 0)
    def _():
        rank = bq_ref.shape[1]
        query = dot(cq_ref[...], bq_ref[...], (((1,), (0,)), ((), ())))
        key = dot(ck_ref[...], bk_ref[...], (((1,), (0,)), ((), ())))
        is_query = core[0] == 0
        own_high, own_low = halves(jnp.where(is_query, query, key))
        own_ref[:, :rank] = own_high
        own_ref[:, rank:] = own_low
        other_high, other_low = halves(jnp.where(is_query, key, query))
        other_ref[:, :rank] = other_high
        other_ref[:, rank:] = other_low

    store_block(x_ref, other_ref[...], out_ref)


def own_kernel(own_ref, x_ref, out_ref):
    store_block(x_ref, own_ref[...], out_ref)


def last_kernel(
    core, squares_ref, tiles_ref, mean_ref, square_ref, bq_ref, bk_ref, wq_ref, wk_ref,
    qs_ref, ks_ref, qu_ref, ku_ref, qc_ref, kc_ref, mean_out, square_out, *, entry_count,
):
    total = jnp.sum(squares_ref[...].reshape(-1, squares_ref.shape[-1]), axis=0, keepdims=True)
    total = jnp.sum(total, axis=1, keepdims=True)
    scale = lax.rsqrt(total / entry_count + EPSILON)
    groups = tiles_ref.shape[0] // 2
    mine = groups // 2
    rows, rank = mean_ref.shape[1], mean_ref.shape[2]
    for which, basis, weight, step_ref, up_ref, copy_ref in (
        (0, bq_ref, wq_ref, qs_ref, qu_ref, qc_ref),
        (1, bk_ref, wk_ref, ks_ref, ku_ref, kc_ref),
    ):
        tile = tiles_ref[pl.ds(which * groups + core[0] * mine, mine)].reshape(rows, rank)
        normalized = tile * scale
        mean = BETA_MEAN * mean_ref[which] + (1.0 - BETA_MEAN) * normalized
        square = BETA_SQUARE * square_ref[which] + (1.0 - BETA_SQUARE) * normalized * normalized
        mean_out[which] = mean
        square_out[which] = square
        direction = mean / jnp.sqrt(square)
        step = dot(direction, basis[...].astype(jnp.float32), OUTER, HIGHEST)
        step_ref[...] = step
        updated = weight[...] - STEP_RATE * step
        up_ref[...] = updated
        copy_ref[...] = updated.astype(jnp.bfloat16)


def whole(shape):
    return pl.BlockSpec(shape, lambda *i: (0,) * len(shape))


def local(
    normed_input,
    query_cotangent,
    key_cotangent,
    query_weight,
    key_weight,
    query_basis,
    key_basis,
    moment_mean,
    moment_square,
):
    far, near, cores, heads = (lax.axis_size(a) for a in ("fs_0", "fs_1", "fs_2", "tp"))
    core = lax.axis_index("fs_2").astype(jnp.int32).reshape(1)
    tokens, width = normed_input.shape
    rank = query_basis.shape[1]
    tile = width // (far * near * heads)
    planes = BLOCK // (width // far)
    sums = jax.ShapeDtypeStruct((near * heads, far, tile, rank), jnp.float32)
    x_spec = pl.BlockSpec((tokens, BLOCK), lambda i, *_: (0, i))
    out_spec = pl.BlockSpec((near * heads, planes, tile, rank), lambda i, *_: (0, i, 0, 0))
    cost = pl.CostEstimate(
        flops=4 * tokens * width * rank, bytes_accessed=2 * tokens * width + 4 * width * rank, transcendentals=0
    )
    factor = jax.ShapeDtypeStruct((tokens, 2 * rank), jnp.bfloat16)
    other, own_factor = pl.pallas_call(
        other_kernel,
        grid_spec=pltpu.PrefetchScalarGridSpec(
            num_scalar_prefetch=1,
            grid=(width // BLOCK,),
            in_specs=[
                whole(query_cotangent.shape),
                whole(key_cotangent.shape),
                whole(query_basis.shape),
                whole(key_basis.shape),
                x_spec,
            ],
            out_specs=[out_spec, whole(factor.shape)],
            scratch_shapes=[pltpu.VMEM(factor.shape, factor.dtype)],
        ),
        out_shape=[sums, factor],
        cost_estimate=cost,
        compiler_params=pltpu.CompilerParams(vmem_limit_bytes=16 << 20),
    )(core, query_cotangent, key_cotangent, query_basis, key_basis, normed_input)
    received = lax.ppermute(other, "fs_2", [(0, 1), (1, 0)])
    own = pl.pallas_call(
        own_kernel,
        grid=(width // BLOCK,),
        in_specs=[whole(factor.shape), x_spec],
        out_specs=out_spec,
        out_shape=sums,
        cost_estimate=cost,
        compiler_params=pltpu.CompilerParams(vmem_limit_bytes=16 << 20),
    )(own_factor, normed_input)
    chip = own + received
    plane = jnp.sum(lax.all_to_all(chip, ("fs_1", "tp"), 0, 0, tiled=True), axis=0)
    mine = jnp.sum(lax.all_to_all(plane, "fs_0", 0, 0, tiled=True), axis=0)
    sent = jnp.broadcast_to(mine[None], (cores * heads, tile, rank))
    tiles = lax.all_to_all(sent, ("fs_2", "tp"), 0, 0, tiled=True)
    squares = jnp.sum(tiles * tiles, axis=(0, 1))
    squares = jnp.broadcast_to(squares.reshape(1, 1, rank), (far * near, 1, rank))
    squares = lax.all_to_all(squares, ("fs_0", "fs_1"), 0, 0, tiled=True)
    entry_count = 2.0 * width * rank
    like = lambda a, dtype=None: jax.ShapeDtypeStruct(a.shape, dtype or a.dtype)
    smem = pl.BlockSpec(memory_space=pltpu.SMEM)
    vmem = pl.BlockSpec(memory_space=pltpu.VMEM)
    return pl.pallas_call(
        lambda *refs: last_kernel(*refs, entry_count=entry_count),
        in_specs=[smem] + [vmem] * 8,
        out_specs=[vmem] * 8,
        out_shape=[
            like(query_weight),
            like(key_weight),
            like(query_weight),
            like(key_weight),
            like(query_weight, jnp.bfloat16),
            like(key_weight, jnp.bfloat16),
            like(moment_mean),
            like(moment_square),
        ],
        compiler_params=pltpu.CompilerParams(vmem_limit_bytes=8 << 20),
    )(
        core,
        squares.reshape(far * near, rank),
        tiles,
        moment_mean,
        moment_square,
        query_basis,
        key_basis,
        query_weight,
        key_weight,
    )


def solution(mesh):
    split = Mesh(mesh.devices.reshape(16, 4, 2, mesh.shape["tp"]), ("fs_0", "fs_1", "fs_2", "tp"))
    in_specs = (
        P(FS, None),
        P(FS, "tp"),
        P(FS, "tp"),
        P(FS, "tp"),
        P(FS, "tp"),
        P("tp", None),
        P("tp", None),
        P(None, FS, None),
        P(None, FS, None),
    )
    out_specs = (
        P(FS, "tp"),
        P(FS, "tp"),
        P(FS, "tp"),
        P(FS, "tp"),
        P(FS, "tp"),
        P(FS, "tp"),
        P(None, FS, None),
        P(None, FS, None),
    )
    return jax.shard_map(local, mesh=split, in_specs=in_specs, out_specs=out_specs, check_vma=False)
```

time: 132 us -> 96.7 us (0.73)
  blocking collectives: 113 us -> 72 us
  starting transfers between devices: 0 us -> 8.75 us
  Pallas kernels: 0 us -> 8.62 us
  matrix products: 7.92 us -> 0 us
  other arithmetic: 3.99 us -> 0.22 us
    all_to_all x5 -> x4, blocking collectives: 113 us -> 72 us  [the longest x1 24.4 us: local(): mine = jnp.sum(lax.all_to_all(plane, 'fs_0', 0, 0, tiled=True), axis=0)]
    ppermute x0 -> x1, starting transfers between devices: none -> 8.75 us  [local(): received = lax.ppermute(other, 'fs_2', [(0, 1), (1, 0)])]
    pallas_call x0 -> x3, Pallas kernels: none -> 8.62 us  [the longest x1 3.99 us: local(): pl.pallas_call(other_kernel, grid_spec=pltpu.PrefetchScalarGridSpec(num_s...]
    dot_general x6 -> x0, matrix products: 7.92 us -> none  [the longest x1 3.65 us: local(): lax.dot_general(normed_input, key_cotangent, contract, preferred_element_...]
    unnamed x16 -> x24, local copies, waits for them, and re-layouts: 0.39 us -> 5.81 us
    reduce_sum x6 -> x3, other arithmetic: 3.23 us -> 0.1 us  [the longest x1 0.06 us: local(): jnp.sum(lax.all_to_all(chip, ('fs_1', 'tp'), 0, 0, tiled=True), axis=0)]
    concatenate x1 -> x0, local copies, waits for them, and re-layouts: 1.88 us -> none  [local(): jnp.concatenate([jnp.dot(query_part, query_float, precision=partial_preci...]
    transpose x1 -> x0, local copies, waits for them, and re-layouts: 1.76 us -> none  [cut_along(): return jnp.moveaxis(shard.reshape(*before, size, -1, *after), dim, 0)]
  transfers between devices with their start and end apart: 0 -> 1, of which waited for: 0 -> 0; matrix products, arithmetic and copies ran while one was open for 0% -> 0% of each run, Pallas kernels for 0% -> 4%
where the time goes in v1:
time: 96.7 us; the launch traced here: 96.2 us
  blocking collectives  72 us (74%)
  starting transfers between devices  8.75 us (9%)
  Pallas kernels  8.62 us (9%)
  local copies, waits for them, and re-layouts  5.84 us (6%)
    all_to_all x1, blocking collectives, local(): mine = jnp.sum(lax.all_to_all(plane, 'fs_0', 0, 0, tiled=True), axis=0)  24.4 us
    all_to_all x1, blocking collectives, local(): lax.all_to_all(chip, ('fs_1', 'tp'), 0, 0, tiled=True)  18.8 us
    all_to_all x1, blocking collectives, local(): squares = lax.all_to_all(squares, ('fs_0', 'fs_1'), 0, 0, tiled=True)  17.5 us
    all_to_all x1, blocking collectives, local(): tiles = lax.all_to_all(sent, ('fs_2', 'tp'), 0, 0, tiled=True)  11.2 us
    ppermute x1, starting transfers between devices, local(): received = lax.ppermute(other, 'fs_2', [(0, 1), (1, 0)])  8.75 us
    unnamed x24, local copies, waits for them, and re-layouts  5.81 us
    pallas_call x1, Pallas kernels, local(): pl.pallas_call(other_kernel, grid_spec=pltpu.PrefetchScalarGridSpec(num_s...  3.99 us
    pallas_call x1, Pallas kernels, local(): pl.pallas_call(own_kernel, grid=(width // BLOCK,), in_specs=[whole(factor...  3.58 us
  transfers between devices with their start and end apart: 1, of which 0 were waited for; matrix products, arithmetic and copies ran while one was open for 0% of the time, Pallas kernels for 4%

profile of v1, /device:TPU:1, one launch (start us, length us, event | category | flops | bytes accessed | tf_op | source)
XLA Modules:
  0.0 96.2 jit_solution(1229795628501589373)
XLA Ops:
  0.6 0.0 copy-start
  0.6 2.2 %copy-done = bf16[1024,2048]{1,0:T(8,128)(2,1)S(1)} copy-done((bf16[1024,2048]{1,0:T(8,128)(2,1)S(1)}, bf16[1024,2048]{1,0:T(8,128)(2,1)}, u32[]{:S(2)}) %copy-start) | copy-done | bytes 4194328
  2.8 0.0 copy-start.2
  2.8 1.0 %copy-done.2 = bf16[1024,256]{1,0:T(8,128)(2,1)S(1)} copy-done((bf16[1024,256]{1,0:T(8,128)(2,1)S(1)}, bf16[1024,256]{1,0:T(8,128)(2,1)}, u32[]{:S(2)}) %copy-start.2) | copy-done | bytes 524312
  3.9 0.0 copy-start.3
  3.9 0.8 copy-done.3
  4.7 0.9 copy-done.5
  5.7 0.8 copy-done.6
  6.4 4.0 %shard_map.152 = (f32[16,16,8,128]{3,2,1,0:T(8,128)S(1)}, bf16[1024,256]{1,0:T(8,128)(2,1)S(1)}) custom-call(s32[1]{0:T(128)} %bitcast.core.refs_0_, bf16[1024,256]{1,0:T(8,128)(2,1)S(1)} %copy-done.2, bf16[1024,128]{1,0:T(8,128)(2,1)S(1)} %copy-done.5, bf16[256,128]{1,0:T(8,128)(2,1)S(1)} %copy-done.3, bf16[128,128]{1,0:T(8,128)(2,1)S(1)} %copy-done.6, ...), custom_call_target="tpu_custom_call" | custom-call | flops 1073741824 | bytes 5242880 | tf_op jit(solution)/shard_map/pallas_call | solution.py:119
  10.4 8.7 %collective-permute-start = (f32[16,16,8,128]{3,2,1,0:T(8,128)S(1)}, f32[16,16,8,128]{3,2,1,0:T(8,128)S(1)}, u32[]{:S(2)}, u32[]{:S(2)}) collective-permute-start(f32[16,16,8,128]{3,2,1,0:T(8,128)S(1)} %get-tuple-element.11), channel_id=1, source_target_pairs={{0,4},{4,0},{1,5},{5,1},{2,6},{6,2},{3,7},{7,3},{8,12},{12,8},{9,1... | collective-permute-start | bytes 3145736 | tf_op jit(solution)/shard_map/ppermute | solution.py:138
  19.2 0.0 copy-done.1
  19.2 3.6 %shard_map.153 = f32[16,16,8,128]{3,2,1,0:T(8,128)S(1)} custom-call(bf16[1024,256]{1,0:T(8,128)(2,1)S(1)} %get-tuple-element.10.own_ref, bf16[1024,2048]{1,0:T(8,128)(2,1)S(1)} %copy-done.1), custom_call_target="tpu_custom_call" | custom-call | flops 1073741824 | bytes 5242880 | tf_op jit(solution)/shard_map/pallas_call | solution.py:139
  22.8 0.0 copy-start.4
  22.8 0.0 copy-start.7
  22.8 0.0 copy-start.8
  22.8 0.0 copy-start.9
  22.8 0.0 copy-start.10
  22.8 0.0 copy-start.11
  22.8 0.0 collective-permute-done
  22.9 0.1 add.3
  23.0 18.8 %all_to_all.20 = f32[16,16,8,128]{3,2,1,0:T(8,128)S(1)} all-to-all(f32[16,16,8,128]{3,2,1,0:T(8,128)S(1)} %add.3), channel_id=1, replica_groups=mesh['fs_0'=16,'fs_1'=4,'fs_2'=2,'tp'=4] {'fs_1','tp'}, dimensions={0} | all-to-all | bytes 2097152 | tf_op jit(solution)/shard_map/all_to_all | solution.py:149
  41.8 0.1 reduce_sum.27
  41.9 24.4 %all_to_all.21 = f32[16,8,128]{2,1,0:T(8,128)S(1)} all-to-all(f32[16,8,128]{2,1,0:T(8,128)S(1)} %reduce_sum.27), channel_id=1, replica_groups=mesh['fs_0'=16,'fs_1'=4,'fs_2'=2,'tp'=4] {'fs_0'}, dimensions={0} | all-to-all | bytes 131072 | tf_op jit(solution)/shard_map/all_to_all | solution.py:150
  66.3 11.2 %all_to_all.22.refs_2_ = f32[8,8,128]{2,1,0:T(8,128)S(1)} all-to-all(f32[8,8,128]{2,1,0:T(8,128)S(1)} %broadcast_in_dim.4), channel_id=1, replica_groups=mesh['fs_0'=16,'fs_1'=4,'fs_2'=2,'tp'=4] {'fs_2','tp'}, dimensions={0} | all-to-all | bytes 65536 | tf_op jit(solution)/shard_map/all_to_all | solution.py:152
  77.6 17.5 %all_to_all.23 = f32[64,1,128]{2,1,0:T(1,128)S(1)} all-to-all(f32[64,1,128]{2,1,0:T(1,128)S(1)} %broadcast_in_dim.5), channel_id=1, replica_groups=mesh['fs_0'=16,'fs_1'=4,'fs_2'=2,'tp'=4] {'fs_0','fs_1'}, dimensions={0} | all-to-all | bytes 65536 | tf_op jit(solution)/shard_map/all_to_all | solution.py:155
  95.1 0.0 copy-done.4
  95.1 0.0 copy-done.7
  95.1 0.0 copy-done.8
  95.1 0.0 copy-done.9
  95.1 0.0 copy-done.10
  95.2 0.0 copy-done.11
  95.2 1.0 %shard_map.154 = (f32[16,256]{1,0:T(8,128)}, f32[16,128]{1,0:T(8,128)}, f32[16,256]{1,0:T(8,128)}, f32[16,128]{1,0:T(8,128)}, bf16[16,256]{1,0:T(8,128)(2,1)}, /...) custom-call(s32[1]{0:T(128)} %bitcast.core.refs_0_, f32[64,128]{1,0:T(8,128)S(1)} %bitcast.2, ...), custom_call_target="tpu_custom_call" | custom-call | tf_op jit(solution)/shard_map/pallas_call | solution.py:160
  (7 shorter events, 0.1 us)
Async XLA Ops:
  0.6 2.2 %copy-start = (bf16[1024,2048]{1,0:T(8,128)(2,1)S(1)}, bf16[1024,2048]{1,0:T(8,128)(2,1)}, u32[]{:S(2)}) copy-start(bf16[1024,2048]{1,0:T(8,128)(2,1)} %x_ref.3) | copy-start | bytes 12582916
  2.8 1.0 %copy-start.2 = (bf16[1024,256]{1,0:T(8,128)(2,1)S(1)}, bf16[1024,256]{1,0:T(8,128)(2,1)}, u32[]{:S(2)}) copy-start(bf16[1024,256]{1,0:T(8,128)(2,1)} %cq_ref.1) | copy-start | bytes 1572868
  3.9 0.8 copy-start.3
  4.7 0.9 copy-start.5
  5.7 0.8 copy-start.6
  6.4 12.8 %copy-start.1 = (bf16[1024,2048]{1,0:T(8,128)(2,1)S(1)}, bf16[1024,2048]{1,0:T(8,128)(2,1)}, u32[]{:S(2)}) copy-start(bf16[1024,2048]{1,0:T(8,128)(2,1)} %x_ref.3) | copy-start | bytes 12582916
  10.4 12.4 %collective-permute-start = (f32[16,16,8,128]{3,2,1,0:T(8,128)S(1)}, f32[16,16,8,128]{3,2,1,0:T(8,128)S(1)}, u32[]{:S(2)}, u32[]{:S(2)}) collective-permute-start(f32[16,16,8,128]{3,2,1,0:T(8,128)S(1)} %get-tuple-element.11), channel_id=1, source_target_pairs={{0,4},{4,0},{1,5},{5,1},{2,6},{6,2},{3,7},{7,3},{8,12},{12,8},{9,1... | collective-permute-start | bytes 3145736 | tf_op jit(solution)/shard_map/ppermute | solution.py:138
  22.8 72.4 %copy-start.4 = (bf16[256,128]{1,0:T(8,128)(2,1)S(1)}, bf16[256,128]{1,0:T(8,128)(2,1)}, u32[]{:S(2)}) copy-start(bf16[256,128]{1,0:T(8,128)(2,1)} %refs_5_.1) | copy-start | bytes 196612
  22.8 72.3 %copy-start.7 = (bf16[128,128]{1,0:T(8,128)(2,1)S(1)}, bf16[128,128]{1,0:T(8,128)(2,1)}, u32[]{:S(2)}) copy-start(bf16[128,128]{1,0:T(8,128)(2,1)} %refs_6_.1) | copy-start | bytes 98308
  22.8 72.3 %copy-start.8 = (f32[2,16,128]{2,1,0:T(8,128)S(1)}, f32[2,16,128]{2,1,0:T(8,128)}, u32[]{:S(2)}) copy-start(f32[2,16,128]{2,1,0:T(8,128)} %refs_3_.1) | copy-start | bytes 49156
  22.8 72.3 %copy-start.9 = (f32[2,16,128]{2,1,0:T(8,128)S(1)}, f32[2,16,128]{2,1,0:T(8,128)}, u32[]{:S(2)}) copy-start(f32[2,16,128]{2,1,0:T(8,128)} %refs_4_.1) | copy-start | bytes 49156
  22.8 72.3 %copy-start.10 = (f32[16,256]{1,0:T(8,128)S(1)}, f32[16,256]{1,0:T(8,128)}, u32[]{:S(2)}) copy-start(f32[16,256]{1,0:T(8,128)} %refs_7_.1) | copy-start | bytes 49156
  22.8 72.3 %copy-start.11 = (f32[16,128]{1,0:T(8,128)S(1)}, f32[16,128]{1,0:T(8,128)}, u32[]{:S(2)}) copy-start(f32[16,128]{1,0:T(8,128)} %refs_8_.1) | copy-start | bytes 24580

commit v2 on v1

--- a/solution.py
+++ b/solution.py
@@ -12,7 +12,7 @@
 BETA_SQUARE = 0.8
 STEP_RATE = 0.25
 EPSILON = 1e-06
-BLOCK = 256
+BLOCK = 512
 
 HIGHEST = lax.Precision.HIGHEST
 OUTER = (((1,), (1,)), ((), ()))
@@ -29,35 +29,53 @@
     return high, low
 
 
-def store_block(x_ref, factor, out_ref):
-    both = dot(x_ref[...], factor, TOKENS_OUT)
+def store_block(x, factor, out_ref, first):
+    both = dot(x, factor, TOKENS_OUT)
     rank = both.shape[1] // 2
     part = both[:, :rank] + both[:, rank:]
-    zs, rows = out_ref.shape[1], out_ref.shape[0] * out_ref.shape[2]
-    for z in range(zs):
-        piece = part[z * rows : (z + 1) * rows]
-        out_ref[:, z, :, :] = piece.reshape(out_ref.shape[0], out_ref.shape[2], rank)
-
-
-def other_kernel(core, cq_ref, ck_ref, bq_ref, bk_ref, x_ref, out_ref, own_ref, other_ref):
-    @pl.when(pl.program_id(0) == 0)
-    def _():
-        rank = bq_ref.shape[1]
-        query = dot(cq_ref[...], bq_ref[...], (((1,), (0,)), ((), ())))
-        key = dot(ck_ref[...], bk_ref[...], (((1,), (0,)), ((), ())))
-        is_query = core[0] == 0
-        own_high, own_low = halves(jnp.where(is_query, query, key))
-        own_ref[:, :rank] = own_high
-        own_ref[:, rank:] = own_low
-        other_high, other_low = halves(jnp.where(is_query, key, query))
-        other_ref[:, :rank] = other_high
-        other_ref[:, rank:] = other_low
-
-    store_block(x_ref, other_ref[...], out_ref)
+    groups, _, tile, _ = out_ref.shape
+    for start in range(0, part.shape[0], groups * tile):
+        piece = part[start : start + groups * tile]
+        out_ref[:, (first + start) // (groups * tile), :, :] = piece.reshape(groups, tile, rank)
+
+
+def other_kernel(
+    core, x_hbm, cq_hbm, ck_hbm, bq_hbm, bk_hbm, out_ref, own_ref, x_ref,
+    cq_ref, ck_ref, bq_ref, bk_ref, other_ref, sems, x_sems,
+):
+    copies = [
+        pltpu.make_async_copy(source, target, sems.at[i])
+        for i, (source, target) in enumerate(
+            ((cq_hbm, cq_ref), (bq_hbm, bq_ref), (ck_hbm, ck_ref), (bk_hbm, bk_ref))
+        )
+    ]
+    width = x_ref.shape[1]
+    columns = [slice(i, i + BLOCK) for i in range(0, width, BLOCK)]
+    blocks = [
+        pltpu.make_async_copy(x_hbm.at[:, c], x_ref.at[:, c], x_sems.at[i]) for i, c in enumerate(columns)
+    ]
+    for copy in copies + blocks:
+        copy.start()
+    for copy in copies:
+        copy.wait()
+    rank = bq_ref.shape[1]
+    query = dot(cq_ref[...], bq_ref[...], (((1,), (0,)), ((), ())))
+    key = dot(ck_ref[...], bk_ref[...], (((1,), (0,)), ((), ())))
+    is_query = core[0] == 0
+    own_high, own_low = halves(jnp.where(is_query, query, key))
+    own_ref[:, :rank] = own_high
+    own_ref[:, rank:] = own_low
+    other_high, other_low = halves(jnp.where(is_query, key, query))
+    other_ref[:, :rank] = other_high
+    other_ref[:, rank:] = other_low
+    for c, copy in zip(columns, blocks):
+        copy.wait()
+        store_block(x_ref[:, c], other_ref[...], out_ref, c.start)
 
 
 def own_kernel(own_ref, x_ref, out_ref):
-    store_block(x_ref, own_ref[...], out_ref)
+    for start in range(0, x_ref.shape[1], BLOCK):
+        store_block(x_ref[:, start : start + BLOCK], own_ref[...], out_ref, start)
 
 
 def last_kernel(
@@ -108,43 +126,35 @@
     tokens, width = normed_input.shape
     rank = query_basis.shape[1]
     tile = width // (far * near * heads)
-    planes = BLOCK // (width // far)
-    sums = jax.ShapeDtypeStruct((near * heads, far, tile, rank), jnp.float32)
-    x_spec = pl.BlockSpec((tokens, BLOCK), lambda i, *_: (0, i))
-    out_spec = pl.BlockSpec((near * heads, planes, tile, rank), lambda i, *_: (0, i, 0, 0))
+    sums = pltpu.VMEM((near * heads, far, tile, rank), jnp.float32)
     cost = pl.CostEstimate(
         flops=4 * tokens * width * rank, bytes_accessed=2 * tokens * width + 4 * width * rank, transcendentals=0
     )
-    factor = jax.ShapeDtypeStruct((tokens, 2 * rank), jnp.bfloat16)
-    other, own_factor = pl.pallas_call(
+    params = pltpu.CompilerParams(vmem_limit_bytes=16 << 20)
+    factor = pltpu.VMEM((tokens, 2 * rank), jnp.bfloat16)
+    sources = (normed_input, query_cotangent, key_cotangent, query_basis, key_basis)
+    hbm = pl.BlockSpec(memory_space=pltpu.HBM)
+    vmem = pl.BlockSpec(memory_space=pltpu.VMEM)
+    smem = pl.BlockSpec(memory_space=pltpu.SMEM)
+    other, own_factor, held = pl.pallas_call(
         other_kernel,
-        grid_spec=pltpu.PrefetchScalarGridSpec(
-            num_scalar_prefetch=1,
-            grid=(width // BLOCK,),
-            in_specs=[
-                whole(query_cotangent.shape),
-                whole(key_cotangent.shape),
-                whole(query_basis.shape),
-                whole(key_basis.shape),
-                x_spec,
-            ],
-            out_specs=[out_spec, whole(factor.shape)],
-            scratch_shapes=[pltpu.VMEM(factor.shape, factor.dtype)],
-        ),
-        out_shape=[sums, factor],
+        in_specs=[smem] + [hbm] * len(sources),
+        out_specs=[vmem] * 3,
+        out_shape=[sums, factor, pltpu.VMEM(normed_input.shape, normed_input.dtype)],
+        scratch_shapes=[pltpu.VMEM(a.shape, a.dtype) for a in sources[1:3] + sources[3:]]
+        + [factor, pltpu.SemaphoreType.DMA((4,)), pltpu.SemaphoreType.DMA((width // BLOCK,))],
         cost_estimate=cost,
-        compiler_params=pltpu.CompilerParams(vmem_limit_bytes=16 << 20),
-    )(core, query_cotangent, key_cotangent, query_basis, key_basis, normed_input)
+        compiler_params=params,
+    )(core, *(pltpu.with_memory_space_constraint(a, pltpu.HBM) for a in sources))
     received = lax.ppermute(other, "fs_2", [(0, 1), (1, 0)])
     own = pl.pallas_call(
         own_kernel,
-        grid=(width // BLOCK,),
-        in_specs=[whole(factor.shape), x_spec],
-        out_specs=out_spec,
+        in_specs=[vmem] * 2,
+        out_specs=vmem,
         out_shape=sums,
         cost_estimate=cost,
-        compiler_params=pltpu.CompilerParams(vmem_limit_bytes=16 << 20),
-    )(own_factor, normed_input)
+        compiler_params=params,
+    )(own_factor, held)
     chip = own + received
     plane = jnp.sum(lax.all_to_all(chip, ("fs_1", "tp"), 0, 0, tiled=True), axis=0)
     mine = jnp.sum(lax.all_to_all(plane, "fs_0", 0, 0, tiled=True), axis=0)
@@ -155,8 +165,6 @@
     squares = lax.all_to_all(squares, ("fs_0", "fs_1"), 0, 0, tiled=True)
     entry_count = 2.0 * width * rank
     like = lambda a, dtype=None: jax.ShapeDtypeStruct(a.shape, dtype or a.dtype)
-    smem = pl.BlockSpec(memory_space=pltpu.SMEM)
-    vmem = pl.BlockSpec(memory_space=pltpu.VMEM)
     return pl.pallas_call(
         lambda *refs: last_kernel(*refs, entry_count=entry_count),
         in_specs=[smem] + [vmem] * 8,

time: 96.7 us -> 90.5 us (0.936)
  local copies, waits for them, and re-layouts: 5.84 us -> 0.07 us
    unnamed x24 -> x12, local copies, waits for them, and re-layouts: 5.81 us -> 0.04 us
  transfers between devices with their start and end apart: 1 -> 1, of which waited for: 0 -> 1; matrix products, arithmetic and copies ran while one was open for 0% -> 0% of each run, Pallas kernels for 4% -> 1%
where the time goes in v2:
time: 90.5 us; the launch traced here: 90.3 us
  blocking collectives  72 us (80%)
  starting transfers between devices  8.75 us (10%)
  Pallas kernels  7.67 us (8%)
    all_to_all x1, blocking collectives, local(): mine = jnp.sum(lax.all_to_all(plane, 'fs_0', 0, 0, tiled=True), axis=0)  25 us
    all_to_all x1, blocking collectives, local(): lax.all_to_all(chip, ('fs_1', 'tp'), 0, 0, tiled=True)  18.4 us
    all_to_all x1, blocking collectives, local(): squares = lax.all_to_all(squares, ('fs_0', 'fs_1'), 0, 0, tiled=True)  17.6 us
    all_to_all x1, blocking collectives, local(): tiles = lax.all_to_all(sent, ('fs_2', 'tp'), 0, 0, tiled=True)  10.9 us
    ppermute x1, starting transfers between devices, local(): received = lax.ppermute(other, 'fs_2', [(0, 1), (1, 0)])  8.75 us
    pallas_call x1, Pallas kernels, local(): pl.pallas_call(other_kernel, in_specs=[smem] + [hbm] * len(sources), out_...  5.28 us
  transfers between devices with their start and end apart: 1, of which 1 were waited for; matrix products, arithmetic and copies ran while one was open for 0% of the time, Pallas kernels for 1%

profile of v2, /device:TPU:1, one launch (start us, length us, event | category | flops | bytes accessed | tf_op | source)
XLA Modules:
  0.0 90.3 jit_solution(17544577822805124273)
XLA Ops:
  0.6 5.3 %shard_map.152 = (f32[16,16,8,128]{3,2,1,0:T(8,128)S(1)}, bf16[1024,256]{1,0:T(8,128)(2,1)S(1)}, bf16[1024,2048]{1,0:T(8,128)(2,1)S(1)}) custom-call(s32[1]{0:T(128)} %bitcast.core.refs_0_, bf16[1024,2048]{1,0:T(8,128)(2,1)} %x_hbm.1, bf16[1024,256]{1,0:T(8,128)(2,1)} %cq_hbm.1, bf16[1024,128]{1,0:T(8,128)(2,1)} %ck_hbm.1, bf16[256,128]{1,0:T(8,128)(2,1)} %refs_5_.1, ...), custom_call_target="tpu_custom_call" | custom-call | flops 1073741824 | bytes 5242880 | tf_op jit(solution)/shard_map/pallas_call | solution.py:139
  5.9 8.8 %collective-permute-start = (f32[16,16,8,128]{3,2,1,0:T(8,128)S(1)}, f32[16,16,8,128]{3,2,1,0:T(8,128)S(1)}, u32[]{:S(2)}, u32[]{:S(2)}) collective-permute-start(f32[16,16,8,128]{3,2,1,0:T(8,128)S(1)} %get-tuple-element.13), channel_id=1, source_target_pairs={{0,4},{4,0},{1,5},{5,1},{2,6},{6,2},{3,7},{7,3},{8,12},{12,8},{9,1... | collective-permute-start | bytes 3145736 | tf_op jit(solution)/shard_map/ppermute | solution.py:149
  14.7 1.3 %shard_map.153 = f32[16,16,8,128]{3,2,1,0:T(8,128)S(1)} custom-call(bf16[1024,256]{1,0:T(8,128)(2,1)S(1)} %get-tuple-element.11.own_ref, bf16[1024,2048]{1,0:T(8,128)(2,1)S(1)} %get-tuple-element.12.x_ref), custom_call_target="tpu_custom_call" | custom-call | flops 1073741824 | bytes 5242880 | tf_op jit(solution)/shard_map/pallas_call | solution.py:150
  16.0 0.0 copy-start
  16.0 0.0 copy-start.1
  16.1 0.0 copy-start.2
  16.1 0.0 copy-start.3
  16.1 0.0 copy-start.4
  16.1 0.0 copy-start.5
  16.1 0.8 collective-permute-done
  17.0 0.1 add.3
  17.1 18.4 %all_to_all.20 = f32[16,16,8,128]{3,2,1,0:T(8,128)S(1)} all-to-all(f32[16,16,8,128]{3,2,1,0:T(8,128)S(1)} %add.3), channel_id=1, replica_groups=mesh['fs_0'=16,'fs_1'=4,'fs_2'=2,'tp'=4] {'fs_1','tp'}, dimensions={0} | all-to-all | bytes 2097152 | tf_op jit(solution)/shard_map/all_to_all | solution.py:159
  35.5 0.1 reduce_sum.27
  35.6 25.0 %all_to_all.21 = f32[16,8,128]{2,1,0:T(8,128)S(1)} all-to-all(f32[16,8,128]{2,1,0:T(8,128)S(1)} %reduce_sum.27), channel_id=1, replica_groups=mesh['fs_0'=16,'fs_1'=4,'fs_2'=2,'tp'=4] {'fs_0'}, dimensions={0} | all-to-all | bytes 131072 | tf_op jit(solution)/shard_map/all_to_all | solution.py:160
  60.6 10.9 %all_to_all.22.refs_2_ = f32[8,8,128]{2,1,0:T(8,128)S(1)} all-to-all(f32[8,8,128]{2,1,0:T(8,128)S(1)} %broadcast_in_dim.4), channel_id=1, replica_groups=mesh['fs_0'=16,'fs_1'=4,'fs_2'=2,'tp'=4] {'fs_2','tp'}, dimensions={0} | all-to-all | bytes 65536 | tf_op jit(solution)/shard_map/all_to_all | solution.py:162
  71.6 17.6 %all_to_all.23 = f32[64,1,128]{2,1,0:T(1,128)S(1)} all-to-all(f32[64,1,128]{2,1,0:T(1,128)S(1)} %broadcast_in_dim.5), channel_id=1, replica_groups=mesh['fs_0'=16,'fs_1'=4,'fs_2'=2,'tp'=4] {'fs_0','fs_1'}, dimensions={0} | all-to-all | bytes 65536 | tf_op jit(solution)/shard_map/all_to_all | solution.py:165
  89.2 0.0 copy-done
  89.2 0.0 copy-done.1
  89.2 0.0 copy-done.2
  89.2 0.0 copy-done.3
  89.2 0.0 copy-done.4
  89.2 0.0 copy-done.5
  89.2 1.0 %shard_map.154 = (f32[16,256]{1,0:T(8,128)}, f32[16,128]{1,0:T(8,128)}, f32[16,256]{1,0:T(8,128)}, f32[16,128]{1,0:T(8,128)}, bf16[16,256]{1,0:T(8,128)(2,1)}, /...) custom-call(s32[1]{0:T(128)} %bitcast.core.refs_0_, f32[64,128]{1,0:T(8,128)S(1)} %bitcast.2, ...), custom_call_target="tpu_custom_call" | custom-call | tf_op jit(solution)/shard_map/pallas_call | solution.py:168
  (4 shorter events, 0.1 us)
Async XLA Ops:
  5.9 11.0 %collective-permute-start = (f32[16,16,8,128]{3,2,1,0:T(8,128)S(1)}, f32[16,16,8,128]{3,2,1,0:T(8,128)S(1)}, u32[]{:S(2)}, u32[]{:S(2)}) collective-permute-start(f32[16,16,8,128]{3,2,1,0:T(8,128)S(1)} %get-tuple-element.13), channel_id=1, source_target_pairs={{0,4},{4,0},{1,5},{5,1},{2,6},{6,2},{3,7},{7,3},{8,12},{12,8},{9,1... | collective-permute-start | bytes 3145736 | tf_op jit(solution)/shard_map/ppermute | solution.py:149
  16.0 73.2 %copy-start = (bf16[256,128]{1,0:T(8,128)(2,1)S(1)}, bf16[256,128]{1,0:T(8,128)(2,1)}, u32[]{:S(2)}) copy-start(bf16[256,128]{1,0:T(8,128)(2,1)} %refs_5_.1) | copy-start | bytes 196612
  16.0 73.2 %copy-start.1 = (bf16[128,128]{1,0:T(8,128)(2,1)S(1)}, bf16[128,128]{1,0:T(8,128)(2,1)}, u32[]{:S(2)}) copy-start(bf16[128,128]{1,0:T(8,128)(2,1)} %refs_6_.1) | copy-start | bytes 98308
  16.1 73.1 %copy-start.2 = (f32[2,16,128]{2,1,0:T(8,128)S(1)}, f32[2,16,128]{2,1,0:T(8,128)}, u32[]{:S(2)}) copy-start(f32[2,16,128]{2,1,0:T(8,128)} %refs_3_.1) | copy-start | bytes 49156
  16.1 73.1 %copy-start.3 = (f32[2,16,128]{2,1,0:T(8,128)S(1)}, f32[2,16,128]{2,1,0:T(8,128)}, u32[]{:S(2)}) copy-start(f32[2,16,128]{2,1,0:T(8,128)} %refs_4_.1) | copy-start | bytes 49156
  16.1 73.1 %copy-start.4 = (f32[16,256]{1,0:T(8,128)S(1)}, f32[16,256]{1,0:T(8,128)}, u32[]{:S(2)}) copy-start(f32[16,256]{1,0:T(8,128)} %refs_7_.1) | copy-start | bytes 49156
  16.1 73.1 %copy-start.5 = (f32[16,128]{1,0:T(8,128)S(1)}, f32[16,128]{1,0:T(8,128)}, u32[]{:S(2)}) copy-start(f32[16,128]{1,0:T(8,128)} %refs_8_.1) | copy-start | bytes 24580

commit v3 on v2

--- a/solution.py
+++ b/solution.py
@@ -6,13 +6,17 @@
 from jax.sharding import Mesh
 from jax.sharding import PartitionSpec as P
 
-FS = ("fs_0", "fs_1", "fs_2")
+FAR, MIDDLE, NEAR, CHIPS, CORES, HEADS = "z_far", "z_middle", "z_near", "x", "core", "tp"
+SIZES = (4, 2, 2, 4, 2)
+FS = (FAR, MIDDLE, NEAR, CHIPS, CORES)
 
 BETA_MEAN = 0.75
 BETA_SQUARE = 0.8
 STEP_RATE = 0.25
 EPSILON = 1e-06
-BLOCK = 512
+BLOCK = 1024
+OWN_BLOCK = 512
+PIECES = 4
 
 HIGHEST = lax.Precision.HIGHEST
 OUTER = (((1,), (1,)), ((), ()))
@@ -33,10 +37,12 @@
     both = dot(x, factor, TOKENS_OUT)
     rank = both.shape[1] // 2
     part = both[:, :rank] + both[:, rank:]
-    groups, _, tile, _ = out_ref.shape
+    near, groups, middle, _, tile, _ = out_ref.shape
     for start in range(0, part.shape[0], groups * tile):
+        plane = (first + start) // (groups * tile)
         piece = part[start : start + groups * tile]
-        out_ref[:, (first + start) // (groups * tile), :, :] = piece.reshape(groups, tile, rank)
+        far = plane // (near * middle)
+        out_ref[plane % near, :, plane // near % middle, far, :, :] = piece.reshape(groups, tile, rank)
 
 
 def other_kernel(
@@ -49,11 +55,9 @@
             ((cq_hbm, cq_ref), (bq_hbm, bq_ref), (ck_hbm, ck_ref), (bk_hbm, bk_ref))
         )
     ]
-    width = x_ref.shape[1]
-    columns = [slice(i, i + BLOCK) for i in range(0, width, BLOCK)]
-    blocks = [
-        pltpu.make_async_copy(x_hbm.at[:, c], x_ref.at[:, c], x_sems.at[i]) for i, c in enumerate(columns)
-    ]
+    tokens, width = x_ref.shape
+    rows = [pl.ds(i, tokens // PIECES) for i in range(0, tokens, tokens // PIECES)]
+    blocks = [pltpu.make_async_copy(x_hbm.at[r], x_ref.at[r], x_sems.at[i]) for i, r in enumerate(rows)]
     for copy in copies + blocks:
         copy.start()
     for copy in copies:
@@ -68,14 +72,15 @@
     other_high, other_low = halves(jnp.where(is_query, key, query))
     other_ref[:, :rank] = other_high
     other_ref[:, rank:] = other_low
-    for c, copy in zip(columns, blocks):
+    for copy in blocks:
         copy.wait()
-        store_block(x_ref[:, c], other_ref[...], out_ref, c.start)
+    for start in range(0, width, BLOCK):
+        store_block(x_ref[:, start : start + BLOCK], other_ref[...], out_ref, start)
 
 
 def own_kernel(own_ref, x_ref, out_ref):
-    for start in range(0, x_ref.shape[1], BLOCK):
-        store_block(x_ref[:, start : start + BLOCK], own_ref[...], out_ref, start)
+    for start in range(0, x_ref.shape[1], OWN_BLOCK):
+        store_block(x_ref[:, start : start + OWN_BLOCK], own_ref[...], out_ref, start)
 
 
 def last_kernel(
@@ -92,7 +97,7 @@
         (0, bq_ref, wq_ref, qs_ref, qu_ref, qc_ref),
         (1, bk_ref, wk_ref, ks_ref, ku_ref, kc_ref),
     ):
-        tile = tiles_ref[pl.ds(which * groups + core[0] * mine, mine)].reshape(rows, rank)
+        tile = tiles_ref[pl.ds(which * groups + core[0] * mine, mine), : rows // mine, :].reshape(rows, rank)
         normalized = tile * scale
         mean = BETA_MEAN * mean_ref[which] + (1.0 - BETA_MEAN) * normalized
         square = BETA_SQUARE * square_ref[which] + (1.0 - BETA_SQUARE) * normalized * normalized
@@ -121,12 +126,14 @@
     moment_mean,
     moment_square,
 ):
-    far, near, cores, heads = (lax.axis_size(a) for a in ("fs_0", "fs_1", "fs_2", "tp"))
-    core = lax.axis_index("fs_2").astype(jnp.int32).reshape(1)
+    far, middle, near, chips, cores, heads = (
+        lax.axis_size(a) for a in (FAR, MIDDLE, NEAR, CHIPS, CORES, HEADS)
+    )
+    core = lax.axis_index(CORES).astype(jnp.int32).reshape(1)
     tokens, width = normed_input.shape
     rank = query_basis.shape[1]
-    tile = width // (far * near * heads)
-    sums = pltpu.VMEM((near * heads, far, tile, rank), jnp.float32)
+    tile = width // (far * middle * near * chips * heads)
+    sums = pltpu.VMEM((near, chips * heads, middle, far, tile, rank), jnp.float32)
     cost = pl.CostEstimate(
         flops=4 * tokens * width * rank, bytes_accessed=2 * tokens * width + 4 * width * rank, transcendentals=0
     )
@@ -142,11 +149,11 @@
         out_specs=[vmem] * 3,
         out_shape=[sums, factor, pltpu.VMEM(normed_input.shape, normed_input.dtype)],
         scratch_shapes=[pltpu.VMEM(a.shape, a.dtype) for a in sources[1:3] + sources[3:]]
-        + [factor, pltpu.SemaphoreType.DMA((4,)), pltpu.SemaphoreType.DMA((width // BLOCK,))],
+        + [factor, pltpu.SemaphoreType.DMA((4,)), pltpu.SemaphoreType.DMA((PIECES,))],
         cost_estimate=cost,
         compiler_params=params,
     )(core, *(pltpu.with_memory_space_constraint(a, pltpu.HBM) for a in sources))
-    received = lax.ppermute(other, "fs_2", [(0, 1), (1, 0)])
+    received = lax.ppermute(other, CORES, [(0, 1), (1, 0)])
     own = pl.pallas_call(
         own_kernel,
         in_specs=[vmem] * 2,
@@ -155,14 +162,18 @@
         cost_estimate=cost,
         compiler_params=params,
     )(own_factor, held)
-    chip = own + received
-    plane = jnp.sum(lax.all_to_all(chip, ("fs_1", "tp"), 0, 0, tiled=True), axis=0)
-    mine = jnp.sum(lax.all_to_all(plane, "fs_0", 0, 0, tiled=True), axis=0)
-    sent = jnp.broadcast_to(mine[None], (cores * heads, tile, rank))
-    tiles = lax.all_to_all(sent, ("fs_2", "tp"), 0, 0, tiled=True)
-    squares = jnp.sum(tiles * tiles, axis=(0, 1))
-    squares = jnp.broadcast_to(squares.reshape(1, 1, rank), (far * near, 1, rank))
-    squares = lax.all_to_all(squares, ("fs_0", "fs_1"), 0, 0, tiled=True)
+    position, received = lax.optimization_barrier((lax.axis_index(FAR), received))
+    chip = (own + received).reshape(near * chips * heads, middle, far, tile, rank)
+    plane = jnp.sum(lax.all_to_all(chip, (NEAR, CHIPS, HEADS), 0, 0, tiled=True), axis=0)
+    sent = jnp.broadcast_to(plane[None], (far, *plane.shape)).reshape(far * middle, far, tile, rank)
+    rows = jnp.sum(lax.all_to_all(sent, (FAR, MIDDLE), 0, 0, tiled=True), axis=0)
+    mine = lax.dynamic_slice(rows, (position, 0, 0), (1, tile, rank), allow_negative_indices=False)[0]
+    sent = jnp.concatenate([mine, jnp.sum(rows * rows, axis=0)], axis=0)
+    sent = jnp.broadcast_to(sent[None], (cores * heads, 2 * tile, rank))
+    tiles = lax.all_to_all(sent, (CORES, HEADS), 0, 0, tiled=True)
+    squares = jnp.sum(tiles[:, tile:], axis=(0, 1))
+    squares = jnp.broadcast_to(squares.reshape(1, 1, rank), (middle * near * chips, 1, rank))
+    squares = lax.all_to_all(squares, (MIDDLE, NEAR, CHIPS), 0, 0, tiled=True)
     entry_count = 2.0 * width * rank
     like = lambda a, dtype=None: jax.ShapeDtypeStruct(a.shape, dtype or a.dtype)
     return pl.pallas_call(
@@ -182,7 +193,7 @@
         compiler_params=pltpu.CompilerParams(vmem_limit_bytes=8 << 20),
     )(
         core,
-        squares.reshape(far * near, rank),
+        squares.reshape(middle * near * chips, rank),
         tiles,
         moment_mean,
         moment_square,
@@ -194,7 +205,7 @@
 
 
 def solution(mesh):
-    split = Mesh(mesh.devices.reshape(16, 4, 2, mesh.shape["tp"]), ("fs_0", "fs_1", "fs_2", "tp"))
+    split = Mesh(mesh.devices.reshape(*SIZES, mesh.shape["tp"]), (*FS, HEADS))
     in_specs = (
         P(FS, None),
         P(FS, "tp"),

time: 90.5 us -> 88.1 us (0.973)
  blocking collectives: 72 us -> 67.4 us
  local copies, waits for them, and re-layouts: 0.07 us -> 4.17 us
  Pallas kernels: 7.67 us -> 6.31 us
    all_to_all x4, blocking collectives: 72 us -> 67.4 us  [the longest x1 27 us: local(): lax.all_to_all(sent, (FAR, MIDDLE), 0, 0, tiled=True)]
    unnamed x12 -> x16, local copies, waits for them, and re-layouts: 0.04 us -> 4.14 us
    pallas_call x1, Pallas kernels: 5.28 us -> 3.95 us  [local(): pl.pallas_call(other_kernel, in_specs=[smem] + [hbm] * len(sources), out_...]
  transfers between devices with their start and end apart: 1 -> 1, of which waited for: 1 -> 0; matrix products, arithmetic and copies ran while one was open for 0% -> 0% of each run, Pallas kernels for 1% -> 2%
where the time goes in v3:
time: 88.1 us; the launch traced here: 87.7 us
  blocking collectives  67.4 us (77%)
  starting transfers between devices  8.74 us (10%)
  Pallas kernels  6.31 us (7%)
  local copies, waits for them, and re-layouts  4.17 us (5%)
    all_to_all x1, blocking collectives, local(): lax.all_to_all(sent, (FAR, MIDDLE), 0, 0, tiled=True)  27 us
    all_to_all x1, blocking collectives, local(): lax.all_to_all(chip, (NEAR, CHIPS, HEADS), 0, 0, tiled=True)  18.6 us
    all_to_all x1, blocking collectives, local(): tiles = lax.all_to_all(sent, (CORES, HEADS), 0, 0, tiled=True)  12.4 us
    all_to_all x1, blocking collectives, local(): squares = lax.all_to_all(squares, (MIDDLE, NEAR, CHIPS), 0, 0, tiled=True)  9.37 us
    ppermute x1, starting transfers between devices, local(): received = lax.ppermute(other, CORES, [(0, 1), (1, 0)])  8.74 us
    unnamed x16, local copies, waits for them, and re-layouts  4.14 us
    pallas_call x1, Pallas kernels, local(): pl.pallas_call(other_kernel, in_specs=[smem] + [hbm] * len(sources), out_...  3.95 us
  transfers between devices with their start and end apart: 1, of which 0 were waited for; matrix products, arithmetic and copies ran while one was open for 0% of the time, Pallas kernels for 2%

profile of v3, /device:TPU:1, one launch (start us, length us, event | category | flops | bytes accessed | tf_op | source)
XLA Modules:
  0.0 87.7 jit_solution(5136104418621636626)
XLA Ops:
  0.6 4.0 %shard_map.152 = (f32[2,16,2,4,8,128]{5,4,3,2,1,0:T(8,128)S(1)}, bf16[1024,256]{1,0:T(8,128)(2,1)S(1)}, bf16[1024,2048]{1,0:T(8,128)(2,1)S(1)}) custom-call(s32[1]{0:T(128)} %bitcast.core.refs_0_, bf16[1024,2048]{1,0:T(8,128)(2,1)} %x_hbm.1, bf16[1024,256]{1,0:T(8,128)(2,1)} %cq_hbm.1, bf16[1024,128]{1,0:T(8,128)(2,1)} %ck_hbm.1, bf16[256,128]{1,0:T(8,128)(2,1)} %refs_5_.1, ...), custom_call_target="tpu_custom_call" | custom-call | flops 1073741824 | bytes 5242880 | tf_op jit(solution)/shard_map/pallas_call | solution.py:146
  4.6 0.0 copy-start
  4.6 1.9 %copy-done = bf16[1024,2048]{1,0:T(8,128)(2,1)} copy-done((bf16[1024,2048]{1,0:T(8,128)(2,1)}, bf16[1024,2048]{1,0:T(8,128)(2,1)S(1)}, u32[]{:S(2)}) %copy-start) | copy-done | bytes 4194328
  6.5 8.7 %collective-permute-start = (f32[2,16,2,4,8,128]{5,4,3,2,1,0:T(8,128)S(1)}, f32[2,16,2,4,8,128]{5,4,3,2,1,0:T(8,128)S(1)}, u32[]{:S(2)}, u32[]{:S(2)}) collective-permute-start(f32[2,16,2,4,8,128]{5,4,3,2,1,0:T(8,128)S(1)} %get-tuple-element.15), channel_id=1, source_target_pairs={{0,4},{4,0},{1,5},{5,1},{2,6},{6,2},{3,7},{7,3},{8,12},{12,8},{9,1... | collective-permute-start | bytes 3145736 | tf_op jit(solution)/shard_map/ppermute | solution.py:156
  15.3 0.0 copy-start.1
  15.3 2.2 %copy-done.1 = bf16[1024,2048]{1,0:T(8,128)(2,1)S(1)} copy-done((bf16[1024,2048]{1,0:T(8,128)(2,1)S(1)}, bf16[1024,2048]{1,0:T(8,128)(2,1)}, u32[]{:S(2)}) %copy-start.1) | copy-done | bytes 4194328
  17.5 1.3 %shard_map.153 = f32[2,16,2,4,8,128]{5,4,3,2,1,0:T(8,128)S(1)} custom-call(bf16[1024,256]{1,0:T(8,128)(2,1)S(1)} %get-tuple-element.13.own_ref, bf16[1024,2048]{1,0:T(8,128)(2,1)S(1)} %copy-done.1), custom_call_target="tpu_custom_call" | custom-call | flops 1073741824 | bytes 5242880 | tf_op jit(solution)/shard_map/pallas_call | solution.py:157
  18.8 0.0 copy-start.2
  18.8 0.0 copy-start.3
  18.8 0.0 copy-start.4
  18.8 0.0 copy-start.5
  18.8 0.0 copy-start.6
  18.9 0.0 copy-start.7
  18.9 0.0 collective-permute-done
  18.9 0.2 add.3
  19.1 18.6 %all_to_all.20 = f32[32,2,4,8,128]{4,3,2,1,0:T(8,128)S(1)} all-to-all(f32[32,2,4,8,128]{4,3,2,1,0:T(8,128)S(1)} %bitcast.7), channel_id=1, replica_groups=mesh['z_far'=4,'z_middle'=2,'z_near'=2,'x'=4,'core'=2,'tp'=4] {'z_near',..., dimensions={0} | all-to-all | bytes 2097152 | tf_op jit(solution)/shard_map/all_to_all | solution.py:167
  37.7 0.1 reduce_sum.36
  37.8 27.0 %all_to_all.21 = f32[8,4,8,128]{3,2,1,0:T(8,128)S(1)} all-to-all(f32[8,4,8,128]{3,2,1,0:T(8,128)S(1)} %bitcast.8), channel_id=1, replica_groups=mesh['z_far'=4,'z_middle'=2,'z_near'=2,'x'=4,'core'=2,'tp'=4] {'z_far','..., dimensions={0} | all-to-all | bytes 262144 | tf_op jit(solution)/shard_map/all_to_all | solution.py:169
  64.8 12.4 %all_to_all.22.refs_2_ = f32[8,16,128]{2,1,0:T(8,128)S(1)} all-to-all(f32[8,16,128]{2,1,0:T(8,128)S(1)} %broadcast_in_dim.7), channel_id=1, replica_groups=mesh['z_far'=4,'z_middle'=2,'z_near'=2,'x'=4,'core'=2,'tp'=4] {'core','tp'}, dimensions={0} | all-to-all | bytes 131072 | tf_op jit(solution)/shard_map/all_to_all | solution.py:173
  77.3 9.4 %all_to_all.23 = f32[16,1,128]{2,1,0:T(1,128)S(1)} all-to-all(f32[16,1,128]{2,1,0:T(1,128)S(1)} %broadcast_in_dim.8), channel_id=1, replica_groups=mesh['z_far'=4,'z_middle'=2,'z_near'=2,'x'=4,'core'=2,'tp'=4] {'z_middle..., dimensions={0} | all-to-all | bytes 16384 | tf_op jit(solution)/shard_map/all_to_all | solution.py:176
  86.7 0.0 copy-done.2
  86.7 0.0 copy-done.3
  86.7 0.0 copy-done.4
  86.7 0.0 copy-done.5
  86.7 0.0 copy-done.6
  86.7 0.0 copy-done.7
  86.7 1.0 %shard_map.154 = (f32[16,256]{1,0:T(8,128)}, f32[16,128]{1,0:T(8,128)}, f32[16,256]{1,0:T(8,128)}, f32[16,128]{1,0:T(8,128)}, bf16[16,256]{1,0:T(8,128)(2,1)}, /...) custom-call(s32[1]{0:T(128)} %bitcast.core.refs_0_, f32[16,128]{1,0:T(8,128)S(1)} %bitcast.6, ...), custom_call_target="tpu_custom_call" | custom-call | tf_op jit(solution)/shard_map/pallas_call | solution.py:179
  (8 shorter events, 0.1 us)
Async XLA Ops:
  4.6 1.9 %copy-start = (bf16[1024,2048]{1,0:T(8,128)(2,1)}, bf16[1024,2048]{1,0:T(8,128)(2,1)S(1)}, u32[]{:S(2)}) copy-start(bf16[1024,2048]{1,0:T(8,128)(2,1)S(1)} %get-tuple-element.14.x_ref) | copy-start | bytes 12582916
  6.5 12.3 %collective-permute-start = (f32[2,16,2,4,8,128]{5,4,3,2,1,0:T(8,128)S(1)}, f32[2,16,2,4,8,128]{5,4,3,2,1,0:T(8,128)S(1)}, u32[]{:S(2)}, u32[]{:S(2)}) collective-permute-start(f32[2,16,2,4,8,128]{5,4,3,2,1,0:T(8,128)S(1)} %get-tuple-element.15), channel_id=1, source_target_pairs={{0,4},{4,0},{1,5},{5,1},{2,6},{6,2},{3,7},{7,3},{8,12},{12,8},{9,1... | collective-permute-start | bytes 3145736 | tf_op jit(solution)/shard_map/ppermute | solution.py:156
  15.3 2.2 %copy-start.1 = (bf16[1024,2048]{1,0:T(8,128)(2,1)S(1)}, bf16[1024,2048]{1,0:T(8,128)(2,1)}, u32[]{:S(2)}) copy-start(bf16[1024,2048]{1,0:T(8,128)(2,1)} %copy-done) | copy-start | bytes 12582916
  18.8 67.9 %copy-start.2 = (bf16[256,128]{1,0:T(8,128)(2,1)S(1)}, bf16[256,128]{1,0:T(8,128)(2,1)}, u32[]{:S(2)}) copy-start(bf16[256,128]{1,0:T(8,128)(2,1)} %refs_5_.1) | copy-start | bytes 196612
  18.8 67.9 %copy-start.3 = (bf16[128,128]{1,0:T(8,128)(2,1)S(1)}, bf16[128,128]{1,0:T(8,128)(2,1)}, u32[]{:S(2)}) copy-start(bf16[128,128]{1,0:T(8,128)(2,1)} %refs_6_.1) | copy-start | bytes 98308
  18.8 67.8 %copy-start.4 = (f32[2,16,128]{2,1,0:T(8,128)S(1)}, f32[2,16,128]{2,1,0:T(8,128)}, u32[]{:S(2)}) copy-start(f32[2,16,128]{2,1,0:T(8,128)} %refs_3_.1) | copy-start | bytes 49156
  18.8 67.8 %copy-start.5 = (f32[2,16,128]{2,1,0:T(8,128)S(1)}, f32[2,16,128]{2,1,0:T(8,128)}, u32[]{:S(2)}) copy-start(f32[2,16,128]{2,1,0:T(8,128)} %refs_4_.1) | copy-start | bytes 49156
  18.8 67.8 %copy-start.6 = (f32[16,256]{1,0:T(8,128)S(1)}, f32[16,256]{1,0:T(8,128)}, u32[]{:S(2)}) copy-start(f32[16,256]{1,0:T(8,128)} %refs_7_.1) | copy-start | bytes 49156
  18.9 67.8 %copy-start.7 = (f32[16,128]{1,0:T(8,128)S(1)}, f32[16,128]{1,0:T(8,128)}, u32[]{:S(2)}) copy-start(f32[16,128]{1,0:T(8,128)} %refs_8_.1) | copy-start | bytes 24580

commit v4 on v3

--- a/solution.py
+++ b/solution.py
@@ -130,6 +130,7 @@
         lax.axis_size(a) for a in (FAR, MIDDLE, NEAR, CHIPS, CORES, HEADS)
     )
     core = lax.axis_index(CORES).astype(jnp.int32).reshape(1)
+    position, core = lax.optimization_barrier((lax.axis_index(FAR), core))
     tokens, width = normed_input.shape
     rank = query_basis.shape[1]
     tile = width // (far * middle * near * chips * heads)
@@ -162,7 +163,6 @@
         cost_estimate=cost,
         compiler_params=params,
     )(own_factor, held)
-    position, received = lax.optimization_barrier((lax.axis_index(FAR), received))
     chip = (own + received).reshape(near * chips * heads, middle, far, tile, rank)
     plane = jnp.sum(lax.all_to_all(chip, (NEAR, CHIPS, HEADS), 0, 0, tiled=True), axis=0)
     sent = jnp.broadcast_to(plane[None], (far, *plane.shape)).reshape(far * middle, far, tile, rank)

time: 88.1 us -> 84.5 us (0.959)
  local copies, waits for them, and re-layouts: 4.17 us -> 0.07 us
    unnamed x16 -> x12, local copies, waits for them, and re-layouts: 4.14 us -> 0.04 us
  transfers between devices with their start and end apart: 1 -> 1, of which waited for: 0 -> 1; matrix products, arithmetic and copies ran while one was open for 0% -> 0% of each run, Pallas kernels for 2% -> 2%
where the time goes in v4:
time: 84.5 us; the launch traced here: 84.2 us
  blocking collectives  67.2 us (80%)
  starting transfers between devices  8.75 us (10%)
  Pallas kernels  6.26 us (7%)
  waiting for transfers between devices  0.85 us (1%)
    all_to_all x1, blocking collectives, local(): lax.all_to_all(sent, (FAR, MIDDLE), 0, 0, tiled=True)  27.4 us
    all_to_all x1, blocking collectives, local(): lax.all_to_all(chip, (NEAR, CHIPS, HEADS), 0, 0, tiled=True)  18.2 us
    all_to_all x1, blocking collectives, local(): tiles = lax.all_to_all(sent, (CORES, HEADS), 0, 0, tiled=True)  11.7 us
    all_to_all x1, blocking collectives, local(): squares = lax.all_to_all(squares, (MIDDLE, NEAR, CHIPS), 0, 0, tiled=True)  9.84 us
    ppermute x1, starting transfers between devices, local(): received = lax.ppermute(other, CORES, [(0, 1), (1, 0)])  8.75 us
    pallas_call x1, Pallas kernels, local(): pl.pallas_call(other_kernel, in_specs=[smem] + [hbm] * len(sources), out_...  3.88 us
  transfers between devices with their start and end apart: 1, of which 1 were waited for; matrix products, arithmetic and copies ran while one was open for 0% of the time, Pallas kernels for 2%

profile of v4, /device:TPU:1, one launch (start us, length us, event | category | flops | bytes accessed | tf_op | source)
XLA Modules:
  0.0 84.2 jit_solution(17021244047984707280)
XLA Ops:
  0.6 3.9 %shard_map.152 = (f32[2,16,2,4,8,128]{5,4,3,2,1,0:T(8,128)S(1)}, bf16[1024,256]{1,0:T(8,128)(2,1)S(1)}, bf16[1024,2048]{1,0:T(8,128)(2,1)S(1)}) custom-call(s32[1]{0:T(128)} %bitcast.core.refs_0_, bf16[1024,2048]{1,0:T(8,128)(2,1)} %x_hbm.1, bf16[1024,256]{1,0:T(8,128)(2,1)} %cq_hbm.1, bf16[1024,128]{1,0:T(8,128)(2,1)} %ck_hbm.1, bf16[256,128]{1,0:T(8,128)(2,1)} %refs_5_.1, ...), custom_call_target="tpu_custom_call" | custom-call | flops 1073741824 | bytes 5242880 | tf_op jit(solution)/shard_map/pallas_call | solution.py:147
  4.5 8.7 %collective-permute-start = (f32[2,16,2,4,8,128]{5,4,3,2,1,0:T(8,128)S(1)}, f32[2,16,2,4,8,128]{5,4,3,2,1,0:T(8,128)S(1)}, u32[]{:S(2)}, u32[]{:S(2)}) collective-permute-start(f32[2,16,2,4,8,128]{5,4,3,2,1,0:T(8,128)S(1)} %get-tuple-element.16), channel_id=1, source_target_pairs={{0,4},{4,0},{1,5},{5,1},{2,6},{6,2},{3,7},{7,3},{8,12},{12,8},{9,1... | collective-permute-start | bytes 3145736 | tf_op jit(solution)/shard_map/ppermute | solution.py:157
  13.3 1.3 %shard_map.153 = f32[2,16,2,4,8,128]{5,4,3,2,1,0:T(8,128)S(1)} custom-call(bf16[1024,256]{1,0:T(8,128)(2,1)S(1)} %get-tuple-element.14.own_ref, bf16[1024,2048]{1,0:T(8,128)(2,1)S(1)} %get-tuple-element.15.x_ref), custom_call_target="tpu_custom_call" | custom-call | flops 1073741824 | bytes 5242880 | tf_op jit(solution)/shard_map/pallas_call | solution.py:158
  14.6 0.0 copy-start
  14.6 0.0 copy-start.1
  14.7 0.0 copy-start.2
  14.7 0.0 copy-start.3
  14.7 0.0 copy-start.4
  14.7 0.0 copy-start.5
  14.7 0.8 %collective-permute-done = f32[2,16,2,4,8,128]{5,4,3,2,1,0:T(8,128)S(1)} collective-permute-done((f32[2,16,2,4,8,128]{5,4,3,2,1,0:T(8,128)S(1)}, f32[2,16,2,4,8,128]{5,4,3,2,1,0:T(8,128)S(1)}, u32[]{:S(2)}, u32[]{:S(2)}) %collective-permute-start) | collective-permute-done | bytes 1048608 | tf_op jit(solution)/shard_map/ppermute | solution.py:157
  15.5 0.2 add.3
  15.8 18.2 %all_to_all.20 = f32[32,2,4,8,128]{4,3,2,1,0:T(8,128)S(1)} all-to-all(f32[32,2,4,8,128]{4,3,2,1,0:T(8,128)S(1)} %bitcast.7), channel_id=1, replica_groups=mesh['z_far'=4,'z_middle'=2,'z_near'=2,'x'=4,'core'=2,'tp'=4] {'z_near',..., dimensions={0} | all-to-all | bytes 2097152 | tf_op jit(solution)/shard_map/all_to_all | solution.py:167
  34.0 0.1 reduce_sum.36
  34.1 27.4 %all_to_all.21 = f32[8,4,8,128]{3,2,1,0:T(8,128)S(1)} all-to-all(f32[8,4,8,128]{3,2,1,0:T(8,128)S(1)} %bitcast.8), channel_id=1, replica_groups=mesh['z_far'=4,'z_middle'=2,'z_near'=2,'x'=4,'core'=2,'tp'=4] {'z_far','..., dimensions={0} | all-to-all | bytes 262144 | tf_op jit(solution)/shard_map/all_to_all | solution.py:169
  61.5 11.7 %all_to_all.22.refs_2_ = f32[8,16,128]{2,1,0:T(8,128)S(1)} all-to-all(f32[8,16,128]{2,1,0:T(8,128)S(1)} %broadcast_in_dim.7), channel_id=1, replica_groups=mesh['z_far'=4,'z_middle'=2,'z_near'=2,'x'=4,'core'=2,'tp'=4] {'core','tp'}, dimensions={0} | all-to-all | bytes 131072 | tf_op jit(solution)/shard_map/all_to_all | solution.py:173
  73.3 9.8 %all_to_all.23 = f32[16,1,128]{2,1,0:T(1,128)S(1)} all-to-all(f32[16,1,128]{2,1,0:T(1,128)S(1)} %broadcast_in_dim.8), channel_id=1, replica_groups=mesh['z_far'=4,'z_middle'=2,'z_near'=2,'x'=4,'core'=2,'tp'=4] {'z_middle..., dimensions={0} | all-to-all | bytes 16384 | tf_op jit(solution)/shard_map/all_to_all | solution.py:176
  83.1 0.0 copy-done
  83.1 0.0 copy-done.1
  83.1 0.0 copy-done.2
  83.1 0.0 copy-done.3
  83.1 0.0 copy-done.4
  83.2 0.0 copy-done.5
  83.2 1.0 %shard_map.154 = (f32[16,256]{1,0:T(8,128)}, f32[16,128]{1,0:T(8,128)}, f32[16,256]{1,0:T(8,128)}, f32[16,128]{1,0:T(8,128)}, bf16[16,256]{1,0:T(8,128)(2,1)}, /...) custom-call(s32[1]{0:T(128)} %bitcast.core.refs_0_, f32[16,128]{1,0:T(8,128)S(1)} %bitcast.6, ...), custom_call_target="tpu_custom_call" | custom-call | tf_op jit(solution)/shard_map/pallas_call | solution.py:179
  (8 shorter events, 0.1 us)
Async XLA Ops:
  4.5 11.0 %collective-permute-start = (f32[2,16,2,4,8,128]{5,4,3,2,1,0:T(8,128)S(1)}, f32[2,16,2,4,8,128]{5,4,3,2,1,0:T(8,128)S(1)}, u32[]{:S(2)}, u32[]{:S(2)}) collective-permute-start(f32[2,16,2,4,8,128]{5,4,3,2,1,0:T(8,128)S(1)} %get-tuple-element.16), channel_id=1, source_target_pairs={{0,4},{4,0},{1,5},{5,1},{2,6},{6,2},{3,7},{7,3},{8,12},{12,8},{9,1... | collective-permute-start | bytes 3145736 | tf_op jit(solution)/shard_map/ppermute | solution.py:157
  14.6 68.5 %copy-start = (bf16[256,128]{1,0:T(8,128)(2,1)S(1)}, bf16[256,128]{1,0:T(8,128)(2,1)}, u32[]{:S(2)}) copy-start(bf16[256,128]{1,0:T(8,128)(2,1)} %refs_5_.1) | copy-start | bytes 196612
  14.6 68.5 %copy-start.1 = (bf16[128,128]{1,0:T(8,128)(2,1)S(1)}, bf16[128,128]{1,0:T(8,128)(2,1)}, u32[]{:S(2)}) copy-start(bf16[128,128]{1,0:T(8,128)(2,1)} %refs_6_.1) | copy-start | bytes 98308
  14.7 68.5 %copy-start.2 = (f32[2,16,128]{2,1,0:T(8,128)S(1)}, f32[2,16,128]{2,1,0:T(8,128)}, u32[]{:S(2)}) copy-start(f32[2,16,128]{2,1,0:T(8,128)} %refs_3_.1) | copy-start | bytes 49156
  14.7 68.5 %copy-start.3 = (f32[2,16,128]{2,1,0:T(8,128)S(1)}, f32[2,16,128]{2,1,0:T(8,128)}, u32[]{:S(2)}) copy-start(f32[2,16,128]{2,1,0:T(8,128)} %refs_4_.1) | copy-start | bytes 49156
  14.7 68.5 %copy-start.4 = (f32[16,256]{1,0:T(8,128)S(1)}, f32[16,256]{1,0:T(8,128)}, u32[]{:S(2)}) copy-start(f32[16,256]{1,0:T(8,128)} %refs_7_.1) | copy-start | bytes 49156
  14.7 68.5 %copy-start.5 = (f32[16,128]{1,0:T(8,128)S(1)}, f32[16,128]{1,0:T(8,128)}, u32[]{:S(2)}) copy-start(f32[16,128]{1,0:T(8,128)} %refs_8_.1) | copy-start | bytes 24580

commit v5 on v4

--- a/solution.py
+++ b/solution.py
@@ -45,8 +45,20 @@
         out_ref[plane % near, :, plane // near % middle, far, :, :] = piece.reshape(groups, tile, rank)
 
 
+def store_factor(is_query, cq_ref, ck_ref, bq_ref, bk_ref, factor_ref):
+    rank = bq_ref.shape[1]
+
+    def store(cotangent, basis):
+        high, low = halves(dot(cotangent[...], basis[...], (((1,), (0,)), ((), ()))))
+        factor_ref[:, :rank] = high
+        factor_ref[:, rank:] = low
+
+    pl.when(is_query)(lambda: store(cq_ref, bq_ref))
+    pl.when(jnp.logical_not(is_query))(lambda: store(ck_ref, bk_ref))
+
+
 def other_kernel(
-    core, x_hbm, cq_hbm, ck_hbm, bq_hbm, bk_hbm, out_ref, own_ref, x_ref,
+    core, x_hbm, cq_hbm, ck_hbm, bq_hbm, bk_hbm, out_ref, x_ref,
     cq_ref, ck_ref, bq_ref, bk_ref, other_ref, sems, x_sems,
 ):
     copies = [
@@ -62,23 +74,15 @@
         copy.start()
     for copy in copies:
         copy.wait()
-    rank = bq_ref.shape[1]
-    query = dot(cq_ref[...], bq_ref[...], (((1,), (0,)), ((), ())))
-    key = dot(ck_ref[...], bk_ref[...], (((1,), (0,)), ((), ())))
-    is_query = core[0] == 0
-    own_high, own_low = halves(jnp.where(is_query, query, key))
-    own_ref[:, :rank] = own_high
-    own_ref[:, rank:] = own_low
-    other_high, other_low = halves(jnp.where(is_query, key, query))
-    other_ref[:, :rank] = other_high
-    other_ref[:, rank:] = other_low
+    store_factor(core[0] != 0, cq_ref, ck_ref, bq_ref, bk_ref, other_ref)
     for copy in blocks:
         copy.wait()
     for start in range(0, width, BLOCK):
         store_block(x_ref[:, start : start + BLOCK], other_ref[...], out_ref, start)
 
 
-def own_kernel(own_ref, x_ref, out_ref):
+def own_kernel(core, x_ref, cq_ref, ck_ref, bq_ref, bk_ref, out_ref, own_ref):
+    store_factor(core[0] == 0, cq_ref, ck_ref, bq_ref, bk_ref, own_ref)
     for start in range(0, x_ref.shape[1], OWN_BLOCK):
         store_block(x_ref[:, start : start + OWN_BLOCK], own_ref[...], out_ref, start)
 
@@ -144,25 +148,25 @@
     hbm = pl.BlockSpec(memory_space=pltpu.HBM)
     vmem = pl.BlockSpec(memory_space=pltpu.VMEM)
     smem = pl.BlockSpec(memory_space=pltpu.SMEM)
-    other, own_factor, held = pl.pallas_call(
+    other, *held = pl.pallas_call(
         other_kernel,
         in_specs=[smem] + [hbm] * len(sources),
-        out_specs=[vmem] * 3,
-        out_shape=[sums, factor, pltpu.VMEM(normed_input.shape, normed_input.dtype)],
-        scratch_shapes=[pltpu.VMEM(a.shape, a.dtype) for a in sources[1:3] + sources[3:]]
-        + [factor, pltpu.SemaphoreType.DMA((4,)), pltpu.SemaphoreType.DMA((PIECES,))],
+        out_specs=[vmem] * (1 + len(sources)),
+        out_shape=[sums] + [pltpu.VMEM(a.shape, a.dtype) for a in sources],
+        scratch_shapes=[factor, pltpu.SemaphoreType.DMA((4,)), pltpu.SemaphoreType.DMA((PIECES,))],
         cost_estimate=cost,
         compiler_params=params,
     )(core, *(pltpu.with_memory_space_constraint(a, pltpu.HBM) for a in sources))
     received = lax.ppermute(other, CORES, [(0, 1), (1, 0)])
     own = pl.pallas_call(
         own_kernel,
-        in_specs=[vmem] * 2,
+        in_specs=[smem] + [vmem] * len(sources),
         out_specs=vmem,
         out_shape=sums,
+        scratch_shapes=[factor],
         cost_estimate=cost,
         compiler_params=params,
-    )(own_factor, held)
+    )(core, *held)
     chip = (own + received).reshape(near * chips * heads, middle, far, tile, rank)
     plane = jnp.sum(lax.all_to_all(chip, (NEAR, CHIPS, HEADS), 0, 0, tiled=True), axis=0)
     sent = jnp.broadcast_to(plane[None], (far, *plane.shape)).reshape(far * middle, far, tile, rank)

time: 84.5 us -> 84.5 us (level)
  no operation moved by 1% of the time
where the time goes in v5:
time: 84.5 us; the launch traced here: 84.2 us
  blocking collectives  67.2 us (80%)
  starting transfers between devices  8.75 us (10%)
  Pallas kernels  6.56 us (8%)
    all_to_all x1, blocking collectives, local(): lax.all_to_all(sent, (FAR, MIDDLE), 0, 0, tiled=True)  27.4 us
    all_to_all x1, blocking collectives, local(): lax.all_to_all(chip, (NEAR, CHIPS, HEADS), 0, 0, tiled=True)  18.3 us
    all_to_all x1, blocking collectives, local(): tiles = lax.all_to_all(sent, (CORES, HEADS), 0, 0, tiled=True)  11.7 us
    all_to_all x1, blocking collectives, local(): squares = lax.all_to_all(squares, (MIDDLE, NEAR, CHIPS), 0, 0, tiled=True)  9.84 us
    ppermute x1, starting transfers between devices, local(): received = lax.ppermute(other, CORES, [(0, 1), (1, 0)])  8.75 us
    pallas_call x1, Pallas kernels, local(): pl.pallas_call(other_kernel, in_specs=[smem] + [hbm] * len(sources), out_...  3.92 us
  transfers between devices with their start and end apart: 1, of which 1 were waited for; matrix products, arithmetic and copies ran while one was open for 0% of the time, Pallas kernels for 2%

profile of v5, /device:TPU:1, one launch (start us, length us, event | category | flops | bytes accessed | tf_op | source)
XLA Modules:
  0.0 84.2 jit_solution(7585049489676132577)
XLA Ops:
  0.6 3.9 %shard_map.152 = (f32[2,16,2,4,8,128]{5,4,3,2,1,0:T(8,128)S(1)}, bf16[1024,2048]{1,0:T(8,128)(2,1)S(1)}, bf16[1024,256]{1,0:T(8,128)(2,1)S(1)}, bf16[1024,128]{1...) custom-call(s32[1]{0:T(128)} %bitcast.core.refs_0_, bf16[1024,2048]{1,0:T(8,128)(2,1)} %x_hbm.1, ...), custom_call_target="tpu_custom_call" | custom-call | flops 1073741824 | bytes 5242880 | tf_op jit(solution)/shard_map/pallas_call | solution.py:151
  4.6 8.8 %collective-permute-start = (f32[2,16,2,4,8,128]{5,4,3,2,1,0:T(8,128)S(1)}, f32[2,16,2,4,8,128]{5,4,3,2,1,0:T(8,128)S(1)}, u32[]{:S(2)}, u32[]{:S(2)}) collective-permute-start(f32[2,16,2,4,8,128]{5,4,3,2,1,0:T(8,128)S(1)} %get-tuple-element.22), channel_id=1, source_target_pairs={{0,4},{4,0},{1,5},{5,1},{2,6},{6,2},{3,7},{7,3},{8,12},{12,8},{9,1... | collective-permute-start | bytes 3145736 | tf_op jit(solution)/shard_map/ppermute | solution.py:160
  13.3 1.6 %shard_map.153 = f32[2,16,2,4,8,128]{5,4,3,2,1,0:T(8,128)S(1)} custom-call(s32[1]{0:T(128)} %bitcast.core.refs_0_, bf16[1024,2048]{1,0:T(8,128)(2,1)S(1)} %get-tuple-element.17.x_ref, bf16[1024,256]{1,0:T(8,128)(2,1)S(1)} %get-tuple-element.18.cq_ref, bf16[1024,128]{1,0:T(8,128)(2,1)S(1)} %get-tuple-element.19.ck_ref, ...), custom_call_target="tpu_custom_call" | custom-call | flops 1073741824 | bytes 5242880 | tf_op jit(solution)/shard_map/pallas_call | solution.py:161
  14.9 0.0 copy-start
  14.9 0.0 copy-start.1
  15.0 0.0 copy-start.2
  15.0 0.0 copy-start.3
  15.0 0.0 copy-start.4
  15.0 0.0 copy-start.5
  15.0 0.6 collective-permute-done
  15.6 0.2 add.3
  15.8 18.3 %all_to_all.20 = f32[32,2,4,8,128]{4,3,2,1,0:T(8,128)S(1)} all-to-all(f32[32,2,4,8,128]{4,3,2,1,0:T(8,128)S(1)} %bitcast.7), channel_id=1, replica_groups=mesh['z_far'=4,'z_middle'=2,'z_near'=2,'x'=4,'core'=2,'tp'=4] {'z_near',..., dimensions={0} | all-to-all | bytes 2097152 | tf_op jit(solution)/shard_map/all_to_all | solution.py:171
  34.1 0.1 reduce_sum.36
  34.2 27.4 %all_to_all.21 = f32[8,4,8,128]{3,2,1,0:T(8,128)S(1)} all-to-all(f32[8,4,8,128]{3,2,1,0:T(8,128)S(1)} %bitcast.8), channel_id=1, replica_groups=mesh['z_far'=4,'z_middle'=2,'z_near'=2,'x'=4,'core'=2,'tp'=4] {'z_far','..., dimensions={0} | all-to-all | bytes 262144 | tf_op jit(solution)/shard_map/all_to_all | solution.py:173
  61.6 11.7 %all_to_all.22.refs_2_ = f32[8,16,128]{2,1,0:T(8,128)S(1)} all-to-all(f32[8,16,128]{2,1,0:T(8,128)S(1)} %broadcast_in_dim.7), channel_id=1, replica_groups=mesh['z_far'=4,'z_middle'=2,'z_near'=2,'x'=4,'core'=2,'tp'=4] {'core','tp'}, dimensions={0} | all-to-all | bytes 131072 | tf_op jit(solution)/shard_map/all_to_all | solution.py:177
  73.3 9.8 %all_to_all.23 = f32[16,1,128]{2,1,0:T(1,128)S(1)} all-to-all(f32[16,1,128]{2,1,0:T(1,128)S(1)} %broadcast_in_dim.8), channel_id=1, replica_groups=mesh['z_far'=4,'z_middle'=2,'z_near'=2,'x'=4,'core'=2,'tp'=4] {'z_middle..., dimensions={0} | all-to-all | bytes 16384 | tf_op jit(solution)/shard_map/all_to_all | solution.py:180
  83.2 0.0 copy-done
  83.2 0.0 copy-done.1
  83.2 0.0 copy-done.2
  83.2 0.0 copy-done.3
  83.2 0.0 copy-done.4
  83.2 0.0 copy-done.5
  83.2 1.0 %shard_map.154 = (f32[16,256]{1,0:T(8,128)}, f32[16,128]{1,0:T(8,128)}, f32[16,256]{1,0:T(8,128)}, f32[16,128]{1,0:T(8,128)}, bf16[16,256]{1,0:T(8,128)(2,1)}, /...) custom-call(s32[1]{0:T(128)} %bitcast.core.refs_0_, f32[16,128]{1,0:T(8,128)S(1)} %bitcast.6, ...), custom_call_target="tpu_custom_call" | custom-call | tf_op jit(solution)/shard_map/pallas_call | solution.py:183
  (8 shorter events, 0.1 us)
Async XLA Ops:
  4.6 11.0 %collective-permute-start = (f32[2,16,2,4,8,128]{5,4,3,2,1,0:T(8,128)S(1)}, f32[2,16,2,4,8,128]{5,4,3,2,1,0:T(8,128)S(1)}, u32[]{:S(2)}, u32[]{:S(2)}) collective-permute-start(f32[2,16,2,4,8,128]{5,4,3,2,1,0:T(8,128)S(1)} %get-tuple-element.22), channel_id=1, source_target_pairs={{0,4},{4,0},{1,5},{5,1},{2,6},{6,2},{3,7},{7,3},{8,12},{12,8},{9,1... | collective-permute-start | bytes 3145736 | tf_op jit(solution)/shard_map/ppermute | solution.py:160
  14.9 68.2 %copy-start = (bf16[256,128]{1,0:T(8,128)(2,1)S(1)}, bf16[256,128]{1,0:T(8,128)(2,1)}, u32[]{:S(2)}) copy-start(bf16[256,128]{1,0:T(8,128)(2,1)} %refs_5_.1) | copy-start | bytes 196612
  14.9 68.2 %copy-start.1 = (bf16[128,128]{1,0:T(8,128)(2,1)S(1)}, bf16[128,128]{1,0:T(8,128)(2,1)}, u32[]{:S(2)}) copy-start(bf16[128,128]{1,0:T(8,128)(2,1)} %refs_6_.1) | copy-start | bytes 98308
  15.0 68.2 %copy-start.2 = (f32[2,16,128]{2,1,0:T(8,128)S(1)}, f32[2,16,128]{2,1,0:T(8,128)}, u32[]{:S(2)}) copy-start(f32[2,16,128]{2,1,0:T(8,128)} %refs_3_.1) | copy-start | bytes 49156
  15.0 68.2 %copy-start.3 = (f32[2,16,128]{2,1,0:T(8,128)S(1)}, f32[2,16,128]{2,1,0:T(8,128)}, u32[]{:S(2)}) copy-start(f32[2,16,128]{2,1,0:T(8,128)} %refs_4_.1) | copy-start | bytes 49156
  15.0 68.2 %copy-start.4 = (f32[16,256]{1,0:T(8,128)S(1)}, f32[16,256]{1,0:T(8,128)}, u32[]{:S(2)}) copy-start(f32[16,256]{1,0:T(8,128)} %refs_7_.1) | copy-start | bytes 49156
  15.0 68.2 %copy-start.5 = (f32[16,128]{1,0:T(8,128)S(1)}, f32[16,128]{1,0:T(8,128)}, u32[]{:S(2)}) copy-start(f32[16,128]{1,0:T(8,128)} %refs_8_.1) | copy-start | bytes 24580
